TPU v7x, 32 devices: a whole 2x2x4 slice. The times are simulated.
32 devices in a mesh: grp: 2 (over y), fs: 8 (over z, core), tp: 2 (over x).
Axes of the slice: x: 2, y: 2, z: 4, core: 2. Of those that a mesh axis runs over, the one named last changes fastest.
Arguments:
- tokens: bfloat16 [3584, 2048], P(('grp', 'fs'), 'tp'), parts along dimension 0, may hold values from -170 to 170
- routes: int32 [3584, 6], P(('grp', 'fs')), parts along dimension 0, may hold values from 0 to 15, all different within a row; in each aligned block of 224 rows (0 to 223, 224 to 447, ...) at most 112 rows name the same one
- route_weights: float32 [3584, 6], P(('grp', 'fs')), parts along dimension 0, may hold values from 0.2 to 1
- norm_gain: float32 [2048], P('fs'), may hold values from 0.1 to 1.9
- gate_experts: float32 [16, 2048, 512], P(None, 'fs', 'tp'), may hold values from -0.125 to 0.125
- up_experts: float32 [16, 2048, 512], P(None, 'fs', 'tp'), may hold values from -0.125 to 0.125
- down_experts: float32 [16, 512, 2048], P(None, 'fs', 'tp'), may hold values from -0.25 to 0.25
- shared_gate: float32 [2048, 512], P('fs', 'tp'), may hold values from -0.125 to 0.125
- shared_up: float32 [2048, 512], P('fs', 'tp'), may hold values from -0.125 to 0.125
- shared_down: float32 [512, 2048], P('fs', 'tp'), may hold values from -0.25 to 0.25
Outputs:
- mixed: bfloat16 [3584, 2048], P(('grp', 'fs'), 'tp'), parts along dimension 0
- gate_ready: bfloat16 [32, 2048, 512], P(('grp', 'fs'), None, 'tp'), parts along dimension 0
- up_ready: bfloat16 [32, 2048, 512], P(('grp', 'fs'), None, 'tp'), parts along dimension 0
- down_ready: bfloat16 [32, 512, 2048], P(('grp', 'fs'), 'tp'), parts along dimension 0
- shared_gate_ready: bfloat16 [4096, 512], P('grp', 'tp'), parts along dimension 0
- shared_up_ready: bfloat16 [4096, 512], P('grp', 'tp'), parts along dimension 0
- shared_down_ready: bfloat16 [1024, 2048], P(('grp', 'tp')), parts along dimension 0
There are 2 independent parts, one for each index of `grp`. A program takes and returns all parts, laid end to end along the dimension named above; an argument that names none is the same for every part. Nothing has to cross between parts.
Inputs may be any that keep to these rules, and one draw needn't show every extreme that they name: `routes`: the 6 experts of a row differ; among the rows of one index of fs no expert is named more than 112 times, a bound that some block reaches.
All inputs are finite; a program needn't handle non-finite values.
Results may differ from a plain program's by a relative error of at most 0.013.
Values may be sent and summed in bfloat16 or wider, within the bound.
A program may use at most 128 MiB of HBM per device.

v0:
```python
import functools

import jax
import jax.numpy as jnp
from jax import lax
from jax.experimental import pallas as pl
from jax.experimental.pallas import tpu as pltpu
from jax.sharding import PartitionSpec as P

MESH = pl.DeviceIdType.MESH


def weights_kernel(sizes, *refs):
    groups, n, tps = sizes
    count = 6
    srcs, outs = refs[:count], refs[count:2 * count]
    local_sem, send_sem, recv_sem, pass_send, pass_recv = refs[2 * count:]
    grp, fs, tp = lax.axis_index("grp"), lax.axis_index("fs"), lax.axis_index("tp")
    band = n // tps

    def at(g, f, t):
        return {"grp": g, "fs": f, "tp": t}

    barrier = pltpu.get_barrier_semaphore()
    for o in range(n):
        for x in range(tps):
            if o or x:
                pl.semaphore_signal(
                    barrier, inc=1, device_id=at(grp, lax.rem(fs + o, n), lax.rem(tp + x, tps)), device_id_type=MESH
                )
    for y in range(1, groups):
        pl.semaphore_signal(barrier, inc=1, device_id=at(lax.rem(grp + y, groups), fs, tp), device_id_type=MESH)
    pl.semaphore_wait(barrier, n * tps - 1 + groups - 1)

    def src_of(k, peer, share):
        held = outs[k].shape[0]
        first = peer * held if srcs[k].shape[0] > held else 0
        if k in (0, 1, 3, 4):
            part = srcs[k].shape[1] // groups
            return srcs[k].at[pl.ds(first, held), pl.ds(pl.multiple_of(share * part, part), part), :]
        part = srcs[k].shape[2] // groups
        return srcs[k].at[pl.ds(first, held), :, pl.ds(pl.multiple_of(share * part, part), part)]

    def dst_of(k, source, source_tp, share):
        if k in (0, 1, 3, 4):
            rows = srcs[k].shape[1]
            part = rows // groups
            return outs[k].at[:, pl.ds(pl.multiple_of(source * rows + share * part, part), part), :]
        rows, cols = srcs[k].shape[1:]
        part = cols // groups
        return outs[k].at[
            :,
            pl.ds(pl.multiple_of(lax.rem(source, band) * rows, rows), rows),
            pl.ds(pl.multiple_of(source_tp * cols + share * part, part), part),
        ]

    def over_fs(k, slot, src, dst, where):
        return pltpu.make_async_remote_copy(
            src_ref=src, dst_ref=dst, send_sem=send_sem.at[k, slot[0]], recv_sem=recv_sem.at[k, slot[1]],
            device_id=where, device_id_type=MESH,
        )

    def over_grp(k, slot, block, y):
        return pltpu.make_async_remote_copy(
            src_ref=block, dst_ref=block, send_sem=pass_send.at[k, slot, y - 1], recv_sem=pass_recv.at[k, slot, y - 1],
            device_id=at(lax.rem(grp + y, groups), fs, tp), device_id_type=MESH,
        )

    home = fs // band
    mine = lax.rem(fs, band) * tps + tp
    kept = home == tp

    def own(k, g):
        return pltpu.make_async_copy(src_of(k, fs, g), dst_of(k, fs, tp, g), local_sem.at[k, g])

    def row_send(k, o):
        peer = lax.rem(fs + o, n)
        return over_fs(k, (o, o), src_of(k, peer, grp), dst_of(k, fs, tp, grp), at(grp, peer, tp))

    def down_send(k, o):
        peer = lax.rem(fs + o, n)
        return over_fs(k, (o, mine), src_of(k, peer, grp), dst_of(k, fs, tp, grp), at(grp, peer, home))

    for k in (0, 1, 2, 3, 4, 5):
        for o in range(1, n):
            (down_send if k in (2, 5) else row_send)(k, o).start()
        if k in (2, 5):
            @pl.when(kept)
            def _():
                for g in range(groups):
                    own(k, g).start()

            @pl.when(jnp.logical_not(kept))
            def _():
                down_send(k, 0).start()
        else:
            for g in range(groups):
                own(k, g).start()

    def row_arrived(k, o):
        source = lax.rem(fs + n - o, n)
        block = dst_of(k, source, tp, grp)
        over_fs(k, (o, o), block, block, at(grp, source, tp)).wait_recv()
        return block

    def down_block(k, q, x, share):
        return dst_of(k, tp * band + q, x, share)

    def is_own(q, x):
        return jnp.logical_and(tp * band + q == fs, tp == x)

    def others(k):
        for q in range(band):
            for x in range(tps):
                yield q, x, q * tps + x

    for k in (0, 1, 2, 3, 4, 5):
        if k in (2, 5):
            for q, x, slot in others(k):
                @pl.when(jnp.logical_not(is_own(q, x)))
                def _():
                    block = down_block(k, q, x, grp)
                    over_fs(k, (0, slot), block, block, at(grp, tp * band + q, x)).wait_recv()
                    for y in range(1, groups):
                        over_grp(k, slot, block, y).start()
        else:
            for o in range(1, n):
                block = row_arrived(k, o)
                for y in range(1, groups):
                    over_grp(k, o, block, y).start()

    for k in (0, 1, 2, 3, 4, 5):
        if k in (2, 5):
            for q, x, slot in others(k):
                @pl.when(jnp.logical_not(is_own(q, x)))
                def _():
                    for y in range(1, groups):
                        over_grp(k, slot, down_block(k, q, x, grp), y).wait_send()
                        over_grp(k, slot, down_block(k, q, x, lax.rem(grp + groups - y, groups)), y).wait_recv()
            for o in range(1, n):
                down_send(k, o).wait_send()

            @pl.when(kept)
            def _():
                for g in range(groups):
                    own(k, g).wait()

            @pl.when(jnp.logical_not(kept))
            def _():
                down_send(k, 0).wait_send()
        else:
            for o in range(1, n):
                source = lax.rem(fs + n - o, n)
                for y in range(1, groups):
                    over_grp(k, o, dst_of(k, source, tp, grp), y).wait_send()
                    over_grp(k, o, dst_of(k, source, tp, lax.rem(grp + groups - y, groups)), y).wait_recv()
                row_send(k, o).wait_send()
            for g in range(groups):
                own(k, g).wait()


def move_weights(sizes, gate, up, down, shared_gate, shared_up, shared_down):
    groups, n, tps = sizes
    held = gate.shape[0] // n

    def rows(a, lead):
        return jax.ShapeDtypeStruct((lead, n * a.shape[1], a.shape[2]), jnp.bfloat16)

    def downs(a, lead):
        return jax.ShapeDtypeStruct((lead, n // tps * a.shape[1], tps * a.shape[2]), jnp.bfloat16)

    return pl.pallas_call(
        functools.partial(weights_kernel, sizes),
        out_shape=(
            rows(gate, held), rows(up, held), downs(down, held),
            rows(shared_gate, 1), rows(shared_up, 1), downs(shared_down, 1),
        ),
        in_specs=[pl.BlockSpec(memory_space=pltpu.VMEM)] * 6,
        out_specs=[pl.BlockSpec(memory_space=pl.ANY)] * 6,
        scratch_shapes=[
            pltpu.SemaphoreType.DMA((6, groups)),
            pltpu.SemaphoreType.DMA((6, n)),
            pltpu.SemaphoreType.DMA((6, n)),
            pltpu.SemaphoreType.DMA((6, n, groups - 1)),
            pltpu.SemaphoreType.DMA((6, n, groups - 1)),
        ],
        compiler_params=pltpu.CompilerParams(
            collective_id=0, has_side_effects=True, vmem_limit_bytes=16 * 1024 * 1024
        ),
        cost_estimate=pl.CostEstimate(flops=400_000_000, bytes_accessed=20_000_000, transcendentals=0),
    )(gate, up, down, shared_gate, shared_up, shared_down)


def combine_kernel(sizes, part, shared, out, near, held, across, summed, far, local_sem, near_s, near_r, x_s, x_r, z_s, z_r):
    _, n, tps = sizes
    chips = n // 2
    grp, fs, tp = lax.axis_index("grp"), lax.axis_index("fs"), lax.axis_index("tp")
    chip, core = fs // 2, lax.rem(fs, 2)
    rows, cols = out.shape
    f32 = jnp.float32
    step = 32

    def sibling():
        return {"grp": grp, "fs": chip * 2 + 1 - core, "tp": tp}

    def x_peer(x):
        return {"grp": grp, "fs": fs, "tp": lax.rem(tp + x, tps)}

    def z_peer(o):
        return {"grp": grp, "fs": lax.rem(chip + o, chips) * 2 + core, "tp": tp}

    barrier = pltpu.get_barrier_semaphore()
    peers = [sibling()] + [x_peer(x) for x in range(1, tps)] + [z_peer(o) for o in range(1, chips)]
    for peer in peers:
        pl.semaphore_signal(barrier, inc=1, device_id=peer, device_id_type=MESH)
    pl.semaphore_wait(barrier, len(peers))

    def near_copy(o):
        return pltpu.make_async_remote_copy(
            src_ref=part.at[lax.rem(chip + o, chips) * 2 + 1 - core], dst_ref=near.at[o],
            send_sem=near_s.at[o], recv_sem=near_r.at[o], device_id=sibling(), device_id_type=MESH,
        )

    def keep_copy(o):
        return pltpu.make_async_copy(part.at[lax.rem(chip + o, chips) * 2 + core], held.at[o], local_sem.at[o])

    def x_copy(o, x):
        there = pl.multiple_of(lax.rem(tp + x, tps) * cols, cols)
        return pltpu.make_async_remote_copy(
            src_ref=held.at[o, :, pl.ds(there, cols)], dst_ref=across.at[x - 1, o],
            send_sem=x_s.at[x - 1, o], recv_sem=x_r.at[x - 1, o], device_id=x_peer(x), device_id_type=MESH,
        )

    def z_copy(o):
        return pltpu.make_async_remote_copy(
            src_ref=summed.at[o], dst_ref=far.at[o], send_sem=z_s.at[o], recv_sem=z_r.at[o],
            device_id=z_peer(o), device_id_type=MESH,
        )

    order = list(range(1, chips)) + [0]
    for o in order:
        near_copy(o).start()
        keep_copy(o).start()
    for o in order:
        near_copy(o).wait_recv()
        keep_copy(o).wait()

        @pl.loop(0, rows // step)
        def _(i):
            r = pl.ds(pl.multiple_of(i * step, step), step)
            total = held[o, r, :].astype(f32) + near[o, r, :].astype(f32)
            if o == 0:
                total = total + shared[r, :]
            held[o, r, :] = total.astype(jnp.bfloat16)

        for x in range(1, tps):
            x_copy(o, x).start()
    here = pl.ds(pl.multiple_of(tp * cols, cols), cols)
    for o in order:
        for x in range(1, tps):
            x_copy(o, x).wait_recv()

        @pl.loop(0, rows // step)
        def _(i):
            r = pl.ds(pl.multiple_of(i * step, step), step)
            total = held[o, r, here].astype(f32)
            for x in range(1, tps):
                total = total + across[x - 1, o, r, :].astype(f32)
            summed[o, r, :] = total.astype(jnp.bfloat16)

        if o:
            z_copy(o).start()
    for o in range(1, chips):
        z_copy(o).wait_recv()

    @pl.loop(0, rows // step)
    def _(i):
        r = pl.ds(pl.multiple_of(i * step, step), step)
        total = summed[0, r, :].astype(f32)
        for o in range(1, chips):
            total = total + far[o, r, :].astype(f32)
        out[r, :] = total.astype(jnp.bfloat16)

    for o in order:
        near_copy(o).wait_send()
        for x in range(1, tps):
            x_copy(o, x).wait_send()
        if o:
            z_copy(o).wait_send()


def combine(sizes, partial, shared_part):
    _, n, tps = sizes
    chips = n // 2
    rows, width = shared_part.shape
    cols = width // tps
    bf16 = jnp.bfloat16
    dma = pltpu.SemaphoreType.DMA
    return pl.pallas_call(
        functools.partial(combine_kernel, sizes),
        out_shape=jax.ShapeDtypeStruct((rows, cols), bf16),
        in_specs=[pl.BlockSpec(memory_space=pl.ANY), pl.BlockSpec(memory_space=pltpu.VMEM)],
        out_specs=pl.BlockSpec(memory_space=pltpu.VMEM),
        scratch_shapes=[
            pltpu.VMEM((chips, rows, width), bf16),
            pltpu.VMEM((chips, rows, width), bf16),
            pltpu.VMEM((tps - 1, chips, rows, cols), bf16),
            pltpu.VMEM((chips, rows, cols), bf16),
            pltpu.VMEM((chips, rows, cols), bf16),
            dma((chips,)), dma((chips,)), dma((chips,)),
            dma((tps - 1, chips)), dma((tps - 1, chips)), dma((chips,)), dma((chips,)),
        ],
        compiler_params=pltpu.CompilerParams(
            collective_id=1, has_side_effects=True, vmem_limit_bytes=min(60, 8 + 16 * chips * rows * width // 2**20 // 2) * 2**20
        ),
        cost_estimate=pl.CostEstimate(flops=200_000_000, bytes_accessed=20_000_000, transcendentals=0),
    )(partial.reshape(n, rows, width), shared_part)


def per_device(
    sizes,
    tokens,
    routes,
    route_weights,
    norm_gain,
    gate_experts,
    up_experts,
    down_experts,
    shared_gate,
    shared_up,
    shared_down,
):
    bf16, f32 = jnp.bfloat16, jnp.float32
    groups, n, tps = sizes
    width = tokens.shape[1] * tps
    experts_all = gate_experts.shape[0]
    held = experts_all // n
    gain_rows = norm_gain[None, :, None]
    moved = move_weights(
        sizes,
        (gate_experts * gain_rows).astype(bf16),
        (up_experts * gain_rows).astype(bf16),
        down_experts.astype(bf16),
        (shared_gate[None] * gain_rows).astype(bf16),
        (shared_up[None] * gain_rows).astype(bf16),
        shared_down[None].astype(bf16),
    )
    gate_local, up_local, down_local, sg, su, sd = moved
    sg, su, sd = sg[0], su[0], sd[0]

    gathered = lax.all_gather(tokens, "tp", axis=1, tiled=True)
    widened = gathered.astype(f32)
    normed = (widened * lax.rsqrt(jnp.mean(widened * widened, axis=1, keepdims=True) + 1e-06)).astype(bf16)
    chosen = routes[:, :, None] == jnp.arange(experts_all, dtype=jnp.int32)[None, None, :]
    per_expert = jnp.sum(jnp.where(chosen, route_weights[:, :, None], 0.0), axis=1)
    high = lax.reduce_precision(per_expert, 8, 7)
    pad = -(2 * experts_all) % 128
    packed = jnp.concatenate(
        [normed, high.astype(bf16), (per_expert - high).astype(bf16), jnp.zeros((normed.shape[0], pad), bf16)], axis=1
    )
    everyone = lax.all_gather(packed, "fs", axis=0, tiled=True)
    rows = everyone[:, :width]
    first = lax.axis_index("fs") * held
    scale = lax.dynamic_slice_in_dim(everyone, width + first, held, 1).astype(f32) + lax.dynamic_slice_in_dim(
        everyone, width + experts_all + first, held, 1
    ).astype(f32)

    def hidden(x, g, u):
        return jax.nn.silu(jnp.dot(x, g, preferred_element_type=f32)) * jnp.dot(x, u, preferred_element_type=f32)

    active = jnp.concatenate(
        [(hidden(rows, gate_local[j], up_local[j]) * scale[:, j:j + 1]).astype(bf16) for j in range(held)], axis=1
    )
    partial = jnp.dot(active, down_local.reshape(-1, width), preferred_element_type=f32).astype(bf16)
    shared_part = jnp.dot(hidden(normed, sg, su).astype(bf16), sd, preferred_element_type=f32)
    mixed = combine(sizes, partial, shared_part)
    return mixed, gate_local, up_local, down_local, sg, su, sd


def solution(mesh):
    sizes = (mesh.shape["grp"], mesh.shape["fs"], mesh.shape["tp"])
    return jax.shard_map(
        functools.partial(per_device, sizes),
        mesh=mesh,
        in_specs=(
            P(("grp", "fs"), "tp"),
            P(("grp", "fs"), None),
            P(("grp", "fs"), None),
            P("fs"),
            P(None, "fs", "tp"),
            P(None, "fs", "tp"),
            P(None, "fs", "tp"),
            P("fs", "tp"),
            P("fs", "tp"),
            P("fs", "tp"),
        ),
        out_specs=(
            P(("grp", "fs"), "tp"),
            P(("grp", "fs"), None, "tp"),
            P(("grp", "fs"), None, "tp"),
            P(("grp", "fs"), "tp", None),
            P("grp", "tp"),
            P("grp", "tp"),
            P(("grp", "tp"), None),
        ),
        check_vma=False,
    )
```

profile of v0, /device:TPU:0, one launch (start us, length us, event | category | flops | bytes accessed | tf_op | source)
XLA Modules:
  0.0 341.3 jit_solution(1599868780212698877)
XLA Ops:
  7.2 0.0 copy-start.12
  7.2 0.0 copy-start.13
  7.2 0.0 all-gather.2.cloned.1.call-start
  7.2 14.4 %all_gather.6 = bf16[224,2048]{1,0:T(8,128)(2,1)S(1)} all-gather(bf16[224,1024]{1,0:T(8,128)(2,1)} %param.10), channel_id=1, replica_groups=mesh['grp'=2,'fs'=8,'tp'=2] {'tp'}, dimensions={1}, use_global_device_ids=true | all-gather | bytes 1376256 | tf_op jit(solution)/shard_map/all_gather | solution.py:351
  21.6 0.3 fusion.26
  21.9 0.2 fusion.27
  22.1 0.0 copy-done.12
  22.2 0.0 copy-done.13
  22.2 0.0 copy-start.10
  22.2 0.1 copy.21
  22.3 0.1 copy.22
  22.5 1.1 concatenate.6
  23.6 0.0 all-gather.2.cloned.1.call-update
  23.6 0.0 copy-start.11
  23.6 0.0 copy-start.14
  23.7 2.6 convert_element_type.60.refs_2_
  26.2 0.0 copy-done.10
  26.2 0.0 copy-done.11
  26.3 0.0 copy-done.14
  26.3 1.1 fusion.47
  27.4 4.5 %multiply_convert_fusion = (bf16[16,256,256]{2,1,0:T(8,128)(2,1)S(1)}, bf16[16,256,256]{2,1,0:T(8,128)(2,1)S(1)}) fusion(f32[16,256,256]{2,1,0:T(8,128)} %param.15, f32[256]{0:T(256)S(1)} %copy-done.14, f32[16,256,256]{2,1,0:T(8,128)} %param.14), kind=kLoop, calls=%fused_computation.9 | loop fusion | flops 4194304 | bytes 12583936 | tf_op jit(solution)/shard_map/convert_element_type | solution.py:342
  31.9 184.9 %shard_map.153 = (bf16[2,2048,256]{2,1,0:T(8,128)(2,1)S(1)}, bf16[2,2048,256]{2,1,0:T(8,128)(2,1)S(1)}, bf16[2,256,2048]{2,1,0:T(8,128)(2,1)S(1)}, bf16[1,2048,2...) custom-call(bf16[16,256,256]{2,1,0:T(8,128)(2,1)S(1)} %get-tuple-element.26.refs_0_, ...), custom_call_target="tpu_custom_call" | custom-call | flops 400000000 | bytes 20000000 | tf_op jit(solution)/shard_map/pallas_call | solution.py:172
  216.8 0.0 copy-start
  216.8 1.0 copy-done
  217.8 0.0 copy-start.2
  217.8 1.0 copy-done.2
  218.7 0.0 copy-start.4
  218.7 1.3 copy-done.4
  220.0 0.0 copy-start.6
  220.1 1.3 copy-done.6
  221.4 0.0 copy-start.8
  221.4 1.3 copy-done.8
  222.7 1.9 fusion.52
  224.6 2.7 fusion.32.shared
  227.3 0.0 all-gather.2.cloned.1.call-done
  227.3 0.0 copy-start.9
  227.3 1.6 convert_add_fusion
  228.9 0.0 slice-start
  228.9 0.8 slice_reduce_fusion.1
  229.8 0.0 copy-done.9
  229.8 0.0 slice-start.1
  229.8 5.5 %fusion.2 = f32[1792,256]{0,1:T(8,128)S(1)} fusion(bf16[1792,2176]{1,0:T(8,128)(2,1)} %all-gather.2.cloned.1.call-done, bf16[2,2048,256]{2,1,0:T(8,128)(2,1)S(1)} %copy-done.9), kind=kOutput, calls=%fused_computation.3 | convolution fusion | flops 1879048192 | bytes 10223616 | tf_op jit(solution)/shard_map/dot_general | solution.py:369
  235.3 0.0 slice-done
  235.3 0.0 slice-done.1
  235.4 0.0 copy-start.7
  235.4 2.1 fusion.6
  237.5 0.0 copy-done.7
  237.5 3.0 fusion.20
  240.5 0.0 copy-start.5
  240.5 2.8 fusion.23
  243.2 0.0 copy-done.5
  243.3 4.3 %convolution_convert_fusion = bf16[1792,2048]{1,0:T(8,128)(2,1)S(1)} fusion(bf16[512,2048]{1,0:T(8,128)(2,1)S(1)} %bitcast.36, bf16[1792,256]{0,1:T(8,128)(2,1)S(1)} %fusion.20, bf16[1792,256]{0,1:T(8,128)(2,1)S(1)} %fusion.23), kind=kOutput, calls=%fused_computation | convolution fusion | flops 3765436416 | bytes 11272192 | tf_op jit(solution)/shard_map/dot_general | solution.py:374
  247.6 78.0 %shard_map.154 = bf16[224,1024]{1,0:T(8,128)(2,1)S(1)} custom-call(bf16[8,224,2048]{2,1,0:T(8,128)(2,1)S(1)} %bitcast.29, f32[224,2048]{1,0:T(8,128)S(1)} %fusion.32.shared), custom_call_target="tpu_custom_call" | custom-call | flops 200000000 | bytes 20000000 | tf_op jit(solution)/shard_map/pallas_call | solution.py:299
  325.5 0.8 copy.30
  326.3 1.3 copy.31
  327.6 1.3 copy.32
  329.0 0.0 copy-start.3
  329.0 1.3 copy.33
  330.3 0.6 copy-done.3
  330.9 0.0 copy-start.1
  330.9 1.0 copy.34
  331.9 0.6 copy-done.1
  332.5 1.0 copy.35
  333.5 1.0 copy.36
  (6 shorter events, 0.1 us)
Async XLA Ops:
  7.2 15.0 %copy-start.12 = (f32[224,6]{0,1:T(8,128)S(1)}, f32[224,6]{0,1:T(8,128)}, u32[]{:S(2)}) copy-start(f32[224,6]{0,1:T(8,128)} %param.12) | copy-start | bytes 16132
  7.2 15.0 %copy-start.13 = (s32[224,6]{0,1:T(8,128)S(1)}, s32[224,6]{0,1:T(8,128)}, u32[]{:S(2)}) copy-start(s32[224,6]{0,1:T(8,128)} %param.11) | copy-start | bytes 16132
  7.2 220.1 %all-gather.2.cloned.1.call-start = ((), (), s32[]{:S(2)}) async-start(), calls=%async_computation | async-start | bytes 8773632 | tf_op jit(solution)/shard_map/all_gather | solution.py:361
  22.2 4.0 %copy-start.10 = (bf16[224,2048]{1,0:T(8,128)(2,1)}, bf16[224,2048]{1,0:T(8,128)(2,1)S(1)}, u32[]{:S(2)}) copy-start(bf16[224,2048]{1,0:T(8,128)(2,1)S(1)} %fusion.27) | copy-start | bytes 2752516
  23.6 2.6 copy-start.11
  23.6 2.6 copy-start.14
  216.8 1.0 copy-start
  217.8 1.0 copy-start.2
  218.7 1.3 copy-start.4
  220.0 1.3 copy-start.6
  221.4 1.3 copy-start.8
  227.3 2.5 copy-start.9
  228.9 6.4 %slice-start = ((s8[7798784]{0:T(1024)(128)(4,1)}), s8[4194304]{0:T(1024)(128)(4,1)S(1)}, s32[]{:S(2)}) async-start(s8[7798784]{0:T(1024)(128)(4,1)} %bitcast.37), calls=%async_computation.1 | async-start | bytes 8388608
  229.8 5.6 %slice-start.1 = ((s8[7798784]{0:T(1024)(128)(4,1)}), s8[3604480]{0:T(1024)(128)(4,1)S(1)}, s32[]{:S(2)}) async-start(s8[7798784]{0:T(1024)(128)(4,1)} %bitcast.37), calls=%async_computation.2 | async-start | bytes 7208960
  235.4 2.1 copy-start.7
  240.5 2.8 copy-start.5
  329.0 2.0 copy-start.3
  330.9 1.6 copy-start.1
Sparse Core Ops, SparseCore 0:
  23.7 159.9 all-gather.1
where the time goes:
time: 342 us; the launch traced here: 341 us
  Pallas kernels  263 us (77%)
  matrix products  22.2 us (6%)
  local copies, waits for them, and re-layouts  17 us (5%)
  blocking collectives  14.4 us (4%)
  between operations  14.4 us (4%)
  other arithmetic  10.3 us (3%)
    pallas_call x1, Pallas kernels, move_weights(): pl.pallas_call(functools.partial(weights_kernel, sizes), out_shape=(rows(...  185 us
    pallas_call x1, Pallas kernels, combine(): pl.pallas_call(functools.partial(combine_kernel, sizes), out_shape=jax.Sh...  78 us
    unnamed x41, local copies, waits for them, and re-layouts  14.8 us
    all_gather x1, blocking collectives, per_device(): gathered = lax.all_gather(tokens, 'tp', axis=1, tiled=True)  14.4 us
    dot_general x3, matrix products, hidden(): jnp.dot(x, g, preferred_element_type=f32)  9.55 us
  transfers between devices with their start and end apart: 1, of which 0 were waited for; matrix products, arithmetic and copies ran while one was open for 4% of the time, Pallas kernels for 54%

commit v1 on v0

v1 whole, which is shorter than its diff:
```python
import functools

import jax
import jax.numpy as jnp
from jax import lax
from jax.experimental import pallas as pl
from jax.experimental.pallas import tpu as pltpu
from jax.sharding import PartitionSpec as P

MESH = pl.DeviceIdType.MESH


def move_kernel(sizes, *refs):
    groups, n, tps = sizes
    chips, band = n // 2, n // tps
    half = band // 2
    tok_in, sc_in = refs[:2]
    srcs = refs[2:8]
    tok, sc = refs[8:10]
    outs = refs[10:16]
    (
        own_s, lz_s, lz_r, ls_s, ls_r, lx_s, lx_r, ly_s, ly_r,
        e_s, e_r, p_s, p_r, d_s, d_r, dy_s, dy_r, ds_s, ds_r,
    ) = refs[16:]
    grp, fs, tp = lax.axis_index("grp"), lax.axis_index("fs"), lax.axis_index("tp")
    z, c = fs // 2, lax.rem(fs, 2)
    home = fs // band
    cols = tok_in.shape[1]
    both = fs + 1 - 2 * c

    def at(g, f, t):
        return {"grp": g, "fs": f, "tp": t}

    def turn(v, by, size):
        return lax.rem(v + by + size, size)

    def remote(src, dst, ssem, rsem, where):
        return pltpu.make_async_remote_copy(
            src_ref=src, dst_ref=dst, send_sem=ssem, recv_sem=rsem, device_id=where, device_id_type=MESH
        )

    def arrived(block, rsem):
        remote(block, block, rsem, rsem, at(grp, both, tp)).wait_recv()

    def span(start, size):
        return pl.ds(pl.multiple_of(start * size, size), size)

    def tok_at(f, x):
        return tok.at[f, :, span(x, cols)]

    own = [
        pltpu.make_async_copy(tok_in, tok_at(fs, tp), own_s.at[0]),
        pltpu.make_async_copy(sc_in, sc.at[fs], own_s.at[1]),
    ]
    for copy in own:
        copy.start()

    barrier = pltpu.get_barrier_semaphore()
    for o in range(n):
        for x in range(tps):
            if o or x:
                pl.semaphore_signal(
                    barrier, inc=1, device_id=at(grp, turn(fs, o, n), turn(tp, x, tps)), device_id_type=MESH
                )
    for y in range(1, groups):
        pl.semaphore_signal(barrier, inc=1, device_id=at(turn(grp, y, groups), fs, tp), device_id_type=MESH)
    pl.semaphore_wait(barrier, n * tps - 1 + groups - 1)

    def line_block(i, f, share):
        if i == 0:
            return tok_at(f, tp)
        if i == 1:
            return sc.at[f]
        rows = srcs[i + 1].shape[1]
        return outs[i + 1].at[0, span(f * groups + share, rows // groups), :]

    def line_source(i):
        if i < 2:
            return line_block(i, fs, grp)
        return srcs[i + 1].at[0, span(grp, srcs[i + 1].shape[1] // groups), :]

    def line_send(i, zs, up, source=None):
        block = line_block(i, zs * 2 + c, grp)
        there = turn(z, 1 if up else -1, chips) * 2 + c
        return remote(
            block if source is None else source, block, lz_s.at[i, up, zs], lz_r.at[i, zs], at(grp, there, tp)
        )

    def x_block(f, v):
        return tok_at(f, turn(tp, -v, tps))

    def x_send(zs, x):
        block = tok_at(zs * 2 + c, tp)
        return remote(block, block, lx_s.at[x - 1, zs], lx_r.at[x - 1, zs], at(grp, fs, turn(tp, x, tps)))

    def y_send(i, zs, y):
        block = line_block(i, zs * 2 + c, grp)
        return remote(
            block, block, ly_s.at[i - 2, y - 1, zs], ly_r.at[i - 2, y - 1, zs], at(turn(grp, y, groups), fs, tp)
        )

    def sib_block(i, f, v):
        return x_block(f, v) if i == 0 else line_block(i, f, turn(grp, -v, groups))

    def sib_send(i, zs, v, source=None):
        block = sib_block(i, zs * 2 + c, v)
        return remote(
            block if source is None else source, block, ls_s.at[i, v, zs], ls_r.at[i, v, zs], at(grp, both, tp)
        )

    def ways(i):
        return (tps, 1, groups, groups)[i]

    def own_share(i, v):
        if i < 2:
            return None
        return srcs[i + 1].at[0, span(turn(grp, -v, groups), srcs[i + 1].shape[1] // groups), :]

    def ends(up):
        return z < chips - 1 if up else z > 0

    def line_own(i):
        for up in (0, 1):
            @pl.when(ends(up))
            def _():
                line_send(i, z, up, line_source(i)).start()

    def line_spread(i, zs):
        if i == 0:
            for x in range(1, tps):
                x_send(zs, x).start()
        sib_send(i, zs, 0).start()
        if i > 1:
            for y in range(1, groups):
                y_send(i, zs, y).start()

    def line_arrivals(i, d):
        for up in (1, 0):
            zs = turn(z, -d if up else d, chips)

            @pl.when(z >= d if up else z + d < chips)
            def _():
                arrived(line_block(i, zs * 2 + c, grp), lz_r.at[i, zs])

                @pl.when(ends(up))
                def _():
                    line_send(i, zs, up).start()

                line_spread(i, zs)

    def held(k):
        return outs[k].shape[0]

    def e_src(k, f, share):
        first = f * held(k)
        if k < 2:
            rows = srcs[k].shape[1]
            at_rows = pl.ds(0, rows) if share is None else span(share, rows // groups)
            return srcs[k].at[pl.ds(first, held(k)), at_rows, :]
        wide = srcs[k].shape[2]
        at_cols = pl.ds(0, wide) if share is None else span(share, wide // groups)
        return srcs[k].at[pl.ds(first, held(k)), :, at_cols]

    def down_block(k, f, x, share):
        rows, wide = srcs[k].shape[1:]
        at_cols = span(x, wide) if share is None else span(x * groups + share, wide // groups)
        return outs[k].at[:, span(lax.rem(f, band), rows), at_cols]

    def e_dst(k, f, x, share):
        if k == 2:
            return down_block(k, f, x, share)
        rows = srcs[k].shape[1]
        at_rows = span(f, rows) if share is None else span(f * groups + share, rows // groups)
        return outs[k].at[:, at_rows, :]

    def e_slot(k, f, x):
        return f if k < 2 else lax.rem(f, band) * tps + x

    def e_send(k, f, share):
        return remote(
            e_src(k, f, share), e_dst(k, fs, tp, share), e_s.at[k, f], e_r.at[k, e_slot(k, fs, tp)],
            at(grp, f, tp if k < 2 else home),
        )

    def e_pass(k, f, x, y):
        block = e_dst(k, f, x, grp)
        slot = e_slot(k, f, x)
        return remote(block, block, p_s.at[k, slot, y - 1], p_r.at[k, slot, y - 1], at(turn(grp, y, groups), fs, tp))

    def far(s):
        low = (z < chips // 2).astype(jnp.int32)
        down = chips - 1 - s
        down = down - (down <= z).astype(jnp.int32)
        upto = s + (s >= z).astype(jnp.int32)
        return low * down + (1 - low) * upto

    def e_arrive(k, f, x, local):
        def take(share):
            block = e_dst(k, f, x, share)
            arrived(block, e_r.at[k, e_slot(k, f, x)])

        if local:
            take(None)
            return
        take(grp)
        for y in range(1, groups):
            e_pass(k, f, x, y).start()

    def e_settle(k, f, x):
        for y in range(1, groups):
            e_pass(k, f, x, y).wait_send()
            arrived(e_dst(k, f, x, turn(grp, -y, groups)), p_r.at[k, e_slot(k, f, x), y - 1])

    def sd_send(zd, share):
        src = srcs[5].at[:, :, :] if share is None else srcs[5].at[:, :, span(share, srcs[5].shape[2] // groups)]
        return remote(
            src, down_block(5, fs, tp, share), d_s.at[zd], d_r.at[lax.rem(z, half), tp], at(grp, zd * 2 + c, home)
        )

    def sd_pass(q, x, y):
        block = down_block(5, (tp * half + q) * 2 + c, x, grp)
        return remote(
            block, block, dy_s.at[q, x, y - 1], dy_r.at[q, x, y - 1], at(turn(grp, y, groups), fs, tp)
        )

    def sd_sib(q, x, v, local, source=None):
        share = None if local else turn(grp, -v, groups)
        block = down_block(5, (tp * half + q) * 2 + c, x, share)
        return remote(
            block if source is None else source, block, ds_s.at[q, x, v], ds_r.at[q, x, v], at(grp, both, tp)
        )

    for copy in own:
        copy.wait()
    for i in (0, 1, 2, 3):
        line_own(i)
    for s in range(chips - 1):
        for k in (0, 1):
            for dc in (0, 1):
                e_send(k, far(s) * 2 + dc, grp).start()
    for k in (0, 1):
        e_send(k, both, None).start()
    for x in range(1, tps):
        x_send(z, x).start()
    for i in (0, 1, 2, 3):
        for v in range(ways(i)):
            if i or not v:
                sib_send(i, z, v, own_share(i, v)).start()

    @pl.when(home == tp)
    def _():
        e_send(2, both, None).start()
        sd_sib(lax.rem(z, half), tp, 0, True, srcs[5].at[:, :, :]).start()

    @pl.when(home != tp)
    def _():
        for dc in (0, 1):
            e_send(2, z * 2 + dc, None).start()
        sd_send(z, None).start()

    for i in (0, 1, 2, 3):
        line_arrivals(i, 1)
    for s in range(chips - 1):
        for dc in (0, 1):
            e_send(2, far(s) * 2 + dc, grp).start()
        sd_send(far(s), grp).start()

    def keep(k, x):
        rows, wide = srcs[k].shape[1:]
        first = fs * held(k) if k < 3 else 0
        for j in range(held(k)):
            if k in (2, 5):
                outs[k][j, span(lax.rem(fs, band), rows), span(x, wide)] = srcs[k][first + j]
            else:
                outs[k][j, span(fs, rows), :] = srcs[k][first + j]

    for k in (0, 1, 3, 4):
        keep(k, tp)

    @pl.when(home == tp)
    def _():
        keep(2, tp)
        keep(5, tp)

    for k in (0, 1):
        for s in range(chips - 1):
            for dc in (0, 1):
                e_arrive(k, far(s) * 2 + dc, tp, False)
    for d in range(2, chips):
        for i in (0, 1, 2, 3):
            line_arrivals(i, d)

    def sd_sources():
        for q in range(half):
            for x in range(tps):
                yield q, x, tp * half + q

    def downs(k):
        for q, x, zs in sd_sources():
            near = zs == z
            cores = (0, 1) if k == 2 else (0,)
            for dc in cores:
                f = zs * 2 + (dc if k == 2 else c)
                yield q, x, near, f

    for q, x, near, f in downs(2):
        @pl.when(jnp.logical_not(near))
        def _():
            e_arrive(2, f, x, False)

        @pl.when(jnp.logical_and(near, jnp.logical_or(f != fs, tp != x)))
        def _():
            e_arrive(2, f, x, True)

    for q, x, near, f in downs(5):
        @pl.when(jnp.logical_not(near))
        def _():
            arrived(down_block(5, f, x, grp), d_r.at[q, x])
            sd_sib(q, x, 0, False).start()
            for y in range(1, groups):
                sd_pass(q, x, y).start()

        @pl.when(jnp.logical_and(near, tp != x))
        def _():
            arrived(down_block(5, f, x, None), d_r.at[q, x])
            sd_sib(q, x, 0, True).start()

    for zs in range(chips):
        for x in range(1, tps):
            arrived(x_block(zs * 2 + c, x), lx_r.at[x - 1, zs])
            sib_send(0, zs, x).start()
    for dz in range(1, chips):
        zs = turn(z, dz, chips)
        for i in (2, 3):
            for y in range(1, groups):
                arrived(sib_block(i, zs * 2 + c, y), ly_r.at[i - 2, y - 1, zs])
                sib_send(i, zs, y).start()
    for q, x, near, f in downs(5):
        @pl.when(jnp.logical_not(near))
        def _():
            for y in range(1, groups):
                arrived(down_block(5, f, x, turn(grp, -y, groups)), dy_r.at[q, x, y - 1])
                sd_sib(q, x, y, False).start()

    for k in (0, 1):
        arrived(e_dst(k, both, tp, None), e_r.at[k, e_slot(k, both, tp)])
        for s in range(chips - 1):
            for dc in (0, 1):
                e_settle(k, far(s) * 2 + dc, tp)
    for q, x, near, f in downs(2):
        @pl.when(jnp.logical_not(near))
        def _():
            e_settle(2, f, x)
    for zs in range(chips):
        for i in (0, 1, 2, 3):
            for v in range(ways(i)):
                arrived(sib_block(i, zs * 2 + 1 - c, v), ls_r.at[i, v, zs])
    for q, x, near, f in downs(5):
        other = f + 1 - 2 * c
        @pl.when(near)
        def _():
            arrived(down_block(5, other, x, None), ds_r.at[q, x, 0])

        @pl.when(jnp.logical_not(near))
        def _():
            for v in range(groups):
                arrived(down_block(5, other, x, turn(grp, -v, groups)), ds_r.at[q, x, v])

    for zs in range(chips):
        for i in (0, 1, 2, 3):
            for v in range(ways(i)):
                sib_send(i, zs, v).wait_send()
        for x in range(1, tps):
            x_send(zs, x).wait_send()
    for dz in range(1, chips):
        for i in (2, 3):
            for y in range(1, groups):
                y_send(i, turn(z, dz, chips), y).wait_send()
    for d in range(chips):
        for up in (0, 1):
            @pl.when(jnp.logical_and(ends(up), z >= d if up else z + d < chips))
            def _():
                for i in (0, 1, 2, 3):
                    line_send(i, turn(z, -d if up else d, chips), up).wait_send()
    for k in (0, 1):
        e_send(k, both, None).wait_send()
    for s in range(chips - 1):
        for k in (0, 1, 2):
            for dc in (0, 1):
                e_send(k, far(s) * 2 + dc, grp).wait_send()
        sd_send(far(s), grp).wait_send()

    @pl.when(home == tp)
    def _():
        e_send(2, both, None).wait_send()

    @pl.when(home != tp)
    def _():
        for dc in (0, 1):
            e_send(2, z * 2 + dc, None).wait_send()
        sd_send(z, None).wait_send()

    for q, x, near, f in downs(5):
        @pl.when(near)
        def _():
            sd_sib(q, x, 0, True).wait_send()

        @pl.when(jnp.logical_not(near))
        def _():
            for v in range(groups):
                sd_sib(q, x, v, False).wait_send()
            for y in range(1, groups):
                sd_pass(q, x, y).wait_send()


def move(sizes, tokens, scales, gate, up, down, shared_gate, shared_up, shared_down):
    groups, n, tps = sizes
    chips = n // 2
    half = n // tps // 2
    held = gate.shape[0] // n
    bf16 = jnp.bfloat16
    ways = max(groups, tps)

    def rows(a, lead):
        return jax.ShapeDtypeStruct((lead, n * a.shape[1], a.shape[2]), bf16)

    def downs(a, lead):
        return jax.ShapeDtypeStruct((lead, n // tps * a.shape[1], tps * a.shape[2]), bf16)

    dma = pltpu.SemaphoreType.DMA
    return pl.pallas_call(
        functools.partial(move_kernel, sizes),
        out_shape=(
            jax.ShapeDtypeStruct((n, tokens.shape[0], tps * tokens.shape[1]), bf16),
            jax.ShapeDtypeStruct((n,) + scales.shape, jnp.float32),
            rows(gate, held), rows(up, held), downs(down, held),
            rows(shared_gate, 1), rows(shared_up, 1), downs(shared_down, 1),
        ),
        in_specs=[pl.BlockSpec(memory_space=pl.ANY)] * 2 + [pl.BlockSpec(memory_space=pltpu.VMEM)] * 6,
        out_specs=[pl.BlockSpec(memory_space=pltpu.VMEM)] * 8,
        scratch_shapes=[
            dma((2,)), dma((4, 2, chips)), dma((4, chips)), dma((4, ways, chips)), dma((4, ways, chips)),
            dma((tps - 1, chips)), dma((tps - 1, chips)), dma((2, groups - 1, chips)), dma((2, groups - 1, chips)),
            dma((3, n)), dma((3, n)), dma((3, n, groups - 1)), dma((3, n, groups - 1)),
            dma((chips,)), dma((half, tps)), dma((half, tps, groups - 1)), dma((half, tps, groups - 1)),
            dma((half, tps, groups)), dma((half, tps, groups)),
        ],
        compiler_params=pltpu.CompilerParams(
            collective_id=0, has_side_effects=True, vmem_limit_bytes=60 * 1024 * 1024
        ),
        cost_estimate=pl.CostEstimate(flops=400_000_000, bytes_accessed=20_000_000, transcendentals=0),
    )(tokens, scales, gate, up, down, shared_gate, shared_up, shared_down)


def combine_kernel(sizes, part, shared, out, near, held, across, summed, far, local_sem, near_s, near_r, x_s, x_r, z_s, z_r):
    _, n, tps = sizes
    chips = n // 2
    grp, fs, tp = lax.axis_index("grp"), lax.axis_index("fs"), lax.axis_index("tp")
    chip, core = fs // 2, lax.rem(fs, 2)
    rows, cols = out.shape
    f32 = jnp.float32
    step = 32

    def sibling():
        return {"grp": grp, "fs": chip * 2 + 1 - core, "tp": tp}

    def x_peer(x):
        return {"grp": grp, "fs": fs, "tp": lax.rem(tp + x, tps)}

    def z_peer(o):
        return {"grp": grp, "fs": lax.rem(chip + o, chips) * 2 + core, "tp": tp}

    barrier = pltpu.get_barrier_semaphore()
    peers = [sibling()] + [x_peer(x) for x in range(1, tps)] + [z_peer(o) for o in range(1, chips)]
    for peer in peers:
        pl.semaphore_signal(barrier, inc=1, device_id=peer, device_id_type=MESH)
    pl.semaphore_wait(barrier, len(peers))

    def near_copy(o):
        return pltpu.make_async_remote_copy(
            src_ref=part.at[lax.rem(chip + o, chips) * 2 + 1 - core], dst_ref=near.at[o],
            send_sem=near_s.at[o], recv_sem=near_r.at[o], device_id=sibling(), device_id_type=MESH,
        )

    def keep_copy(o):
        return pltpu.make_async_copy(part.at[lax.rem(chip + o, chips) * 2 + core], held.at[o], local_sem.at[o])

    def x_copy(o, x):
        there = pl.multiple_of(lax.rem(tp + x, tps) * cols, cols)
        return pltpu.make_async_remote_copy(
            src_ref=held.at[o, :, pl.ds(there, cols)], dst_ref=across.at[x - 1, o],
            send_sem=x_s.at[x - 1, o], recv_sem=x_r.at[x - 1, o], device_id=x_peer(x), device_id_type=MESH,
        )

    def z_copy(o):
        return pltpu.make_async_remote_copy(
            src_ref=summed.at[o], dst_ref=far.at[o], send_sem=z_s.at[o], recv_sem=z_r.at[o],
            device_id=z_peer(o), device_id_type=MESH,
        )

    order = list(range(1, chips)) + [0]
    for o in order:
        near_copy(o).start()
        keep_copy(o).start()
    for o in order:
        near_copy(o).wait_recv()
        keep_copy(o).wait()

        @pl.loop(0, rows // step)
        def _(i):
            r = pl.ds(pl.multiple_of(i * step, step), step)
            total = held[o, r, :].astype(f32) + near[o, r, :].astype(f32)
            if o == 0:
                total = total + shared[r, :]
            held[o, r, :] = total.astype(jnp.bfloat16)

        for x in range(1, tps):
            x_copy(o, x).start()
    here = pl.ds(pl.multiple_of(tp * cols, cols), cols)
    for o in order:
        for x in range(1, tps):
            x_copy(o, x).wait_recv()

        @pl.loop(0, rows // step)
        def _(i):
            r = pl.ds(pl.multiple_of(i * step, step), step)
            total = held[o, r, here].astype(f32)
            for x in range(1, tps):
                total = total + across[x - 1, o, r, :].astype(f32)
            summed[o, r, :] = total.astype(jnp.bfloat16)

        if o:
            z_copy(o).start()
    for o in range(1, chips):
        z_copy(o).wait_recv()

    @pl.loop(0, rows // step)
    def _(i):
        r = pl.ds(pl.multiple_of(i * step, step), step)
        total = summed[0, r, :].astype(f32)
        for o in range(1, chips):
            total = total + far[o, r, :].astype(f32)
        out[r, :] = total.astype(jnp.bfloat16)

    for o in order:
        near_copy(o).wait_send()
        for x in range(1, tps):
            x_copy(o, x).wait_send()
        if o:
            z_copy(o).wait_send()


def combine(sizes, partial, shared_part):
    _, n, tps = sizes
    chips = n // 2
    rows, width = shared_part.shape
    cols = width // tps
    bf16 = jnp.bfloat16
    dma = pltpu.SemaphoreType.DMA
    return pl.pallas_call(
        functools.partial(combine_kernel, sizes),
        out_shape=jax.ShapeDtypeStruct((rows, cols), bf16),
        in_specs=[pl.BlockSpec(memory_space=pl.ANY), pl.BlockSpec(memory_space=pltpu.VMEM)],
        out_specs=pl.BlockSpec(memory_space=pltpu.VMEM),
        scratch_shapes=[
            pltpu.VMEM((chips, rows, width), bf16),
            pltpu.VMEM((chips, rows, width), bf16),
            pltpu.VMEM((tps - 1, chips, rows, cols), bf16),
            pltpu.VMEM((chips, rows, cols), bf16),
            pltpu.VMEM((chips, rows, cols), bf16),
            dma((chips,)), dma((chips,)), dma((chips,)),
            dma((tps - 1, chips)), dma((tps - 1, chips)), dma((chips,)), dma((chips,)),
        ],
        compiler_params=pltpu.CompilerParams(
            collective_id=1, has_side_effects=True, vmem_limit_bytes=min(60, 8 + 16 * chips * rows * width // 2**20 // 2) * 2**20
        ),
        cost_estimate=pl.CostEstimate(flops=200_000_000, bytes_accessed=20_000_000, transcendentals=0),
    )(partial.reshape(n, rows, width), shared_part)


def per_device(
    sizes,
    tokens,
    routes,
    route_weights,
    norm_gain,
    gate_experts,
    up_experts,
    down_experts,
    shared_gate,
    shared_up,
    shared_down,
):
    bf16, f32 = jnp.bfloat16, jnp.float32
    groups, n, tps = sizes
    width = tokens.shape[1] * tps
    experts_all = gate_experts.shape[0]
    held = experts_all // n
    gain_rows = norm_gain[None, :, None]
    chosen = routes[:, :, None] == jnp.arange(experts_all, dtype=jnp.int32)[None, None, :]
    per_expert = jnp.sum(jnp.where(chosen, route_weights[:, :, None], 0.0), axis=1)
    count = tokens.shape[0]
    scales = jnp.pad(per_expert.T, ((0, 0), (0, -count % 128)))
    moved = move(
        sizes,
        tokens,
        scales,
        (gate_experts * gain_rows).astype(bf16),
        (up_experts * gain_rows).astype(bf16),
        down_experts.astype(bf16),
        (shared_gate[None] * gain_rows).astype(bf16),
        (shared_up[None] * gain_rows).astype(bf16),
        shared_down[None].astype(bf16),
    )
    everyone, scales, gate_local, up_local, down_local, sg, su, sd = moved
    sg, su, sd = sg[0], su[0], sd[0]
    here = lax.axis_index("fs")
    widened = everyone.reshape(n * count, width).astype(f32)
    rows = (widened * lax.rsqrt(jnp.mean(widened * widened, axis=1, keepdims=True) + 1e-06)).astype(bf16)
    normed = lax.dynamic_slice_in_dim(rows, here * count, count, 0)
    scale = lax.dynamic_slice_in_dim(scales, here * held, held, 1)[:, :, :count]
    scale = scale.transpose(0, 2, 1).reshape(n * count, held)

    def hidden(x, g, u):
        return jax.nn.silu(jnp.dot(x, g, preferred_element_type=f32)) * jnp.dot(x, u, preferred_element_type=f32)

    active = jnp.concatenate(
        [(hidden(rows, gate_local[j], up_local[j]) * scale[:, j:j + 1]).astype(bf16) for j in range(held)], axis=1
    )
    partial = jnp.dot(active, down_local.reshape(-1, width), preferred_element_type=f32).astype(bf16)
    shared_part = jnp.dot(hidden(normed, sg, su).astype(bf16), sd, preferred_element_type=f32)
    mixed = combine(sizes, partial, shared_part)
    return mixed, gate_local, up_local, down_local, sg, su, sd


def solution(mesh):
    sizes = (mesh.shape["grp"], mesh.shape["fs"], mesh.shape["tp"])
    return jax.shard_map(
        functools.partial(per_device, sizes),
        mesh=mesh,
        in_specs=(
            P(("grp", "fs"), "tp"),
            P(("grp", "fs"), None),
            P(("grp", "fs"), None),
            P("fs"),
            P(None, "fs", "tp"),
            P(None, "fs", "tp"),
            P(None, "fs", "tp"),
            P("fs", "tp"),
            P("fs", "tp"),
            P("fs", "tp"),
        ),
        out_specs=(
            P(("grp", "fs"), "tp"),
            P(("grp", "fs"), None, "tp"),
            P(("grp", "fs"), None, "tp"),
            P(("grp", "fs"), "tp", None),
            P("grp", "tp"),
            P("grp", "tp"),
            P(("grp", "tp"), None),
        ),
        check_vma=False,
    )
```

time: 342 us -> 276 us (0.81)
  Pallas kernels: 263 us -> 210 us
  other arithmetic: 10.3 us -> 28.9 us
  blocking collectives: 14.4 us -> 0 us
  between operations: 14.4 us -> 0.83 us
  local copies, waits for them, and re-layouts: 17 us -> 9.58 us
  matrix products: 22.2 us -> 26.2 us
    pallas_call x1, Pallas kernels: 185 us -> 139 us  [move(): pl.pallas_call(functools.partial(move_kernel, sizes), out_shape=(jax.Shap...]
    all_gather x1 -> x0, blocking collectives: 14.4 us -> none  [per_device(): gathered = lax.all_gather(tokens, 'tp', axis=1, tiled=True)]
    convert_element_type x1, other arithmetic: 0.01 us -> 10.2 us  [per_device(): widened = everyone.reshape(n * count, width).astype(f32)]
    pallas_call x1, Pallas kernels: 78 us -> 70.5 us  [combine(): pl.pallas_call(functools.partial(combine_kernel, sizes), out_shape=jax.Sh...]
    unnamed x41 -> x37, local copies, waits for them, and re-layouts: 14.8 us -> 7.83 us
    reduce_sum x1, other arithmetic: 0.26 us -> 4.58 us  [per_device(): jnp.mean(widened * widened, axis=1, keepdims=True) + 1e-06]
    convert_element_type x1, other arithmetic: 0.22 us -> 4.33 us  [per_device(): (widened * lax.rsqrt(jnp.mean(widened * widened, axis=1, keepdims=True) +...]
  transfers between devices with their start and end apart: 1 -> 0, of which waited for: 0 -> 0; matrix products, arithmetic and copies ran while one was open for 4% -> 0% of each run, Pallas kernels for 54% -> 0%
where the time goes in v1:
time: 276 us
  Pallas kernels  210 us (76%)
  other arithmetic  28.9 us (10%)
  matrix products  26.2 us (9%)
  local copies, waits for them, and re-layouts  9.58 us (3%)
    pallas_call x1, Pallas kernels, move(): pl.pallas_call(functools.partial(move_kernel, sizes), out_shape=(jax.Shap...  139 us
    pallas_call x1, Pallas kernels, combine(): pl.pallas_call(functools.partial(combine_kernel, sizes), out_shape=jax.Sh...  70.5 us
    convert_element_type x1, other arithmetic, per_device(): widened = everyone.reshape(n * count, width).astype(f32)  10.2 us
    dot_general x3, matrix products, hidden(): jnp.dot(x, g, preferred_element_type=f32)  9.82 us
    dot_general x2, matrix products, hidden(): jnp.dot(x, u, preferred_element_type=f32)  8.8 us
    unnamed x37, local copies, waits for them, and re-layouts  7.83 us
    convert_element_type x1, other arithmetic, per_device(): (up_experts * gain_rows).astype(bf16)  6.67 us

profile of v1, /device:TPU:0, one launch (start us, length us, event | category | flops | bytes accessed | tf_op | source)
XLA Modules:
  0.0 275.5 jit_solution(16290934756960025519)
XLA Ops:
  0.6 0.0 copy-start.14
  0.6 0.0 copy-start.11
  0.7 0.0 copy-start.10
  0.7 0.0 copy-start.2
  0.7 6.7 %multiply_convert_fusion.1 = (bf16[16,256,256]{2,1,0:T(8,128)(2,1)}, bf16[16,256,256]{2,1,0:T(8,128)(2,1)}) fusion(f32[16,256,256]{2,1,0:T(8,128)} %param.15, f32[256]{0:T(256)} %param.13, f32[16,256,256]{2,1,0:T(8,128)} %param.14), kind=kLoop, calls=%fused_computation.3 | loop fusion | flops 4194304 | bytes 12583936 | tf_op jit(solution)/shard_map/convert_element_type | solution.py:609
  7.3 0.0 copy-done.14
  7.4 0.0 copy-done.11
  7.4 0.0 copy-done.10
  7.4 0.8 fusion.26
  8.2 0.0 copy-done.2
  8.2 0.0 copy-start.9
  8.2 0.0 copy-start.12
  8.2 0.0 copy-start.13
  8.2 1.7 convert_element_type.64.refs_4_
  9.8 0.0 copy-done.9
  9.8 0.7 convert_bitcast_fusion.refs_7_
  10.5 0.0 copy-done.12
  10.5 0.0 copy-done.13
  10.5 0.6 pad.4.refs_1_
  11.1 139.5 %shard_map.153 = (bf16[8,224,2048]{2,1,0:T(8,128)(2,1)}, f32[8,16,256]{2,1,0:T(8,128)}, bf16[2,2048,256]{2,1,0:T(8,128)(2,1)}, bf16[2,2048,256]{2,1,0:T(8,128)(2...) custom-call(bf16[224,1024]{1,0:T(8,128)(2,1)} %refs_0_.1, ...), custom_call_target="tpu_custom_call" | custom-call | flops 400000000 | bytes 20000000 | tf_op jit(solution)/shard_map/pallas_call | solution.py:431
  150.6 4.6 %multiply_reduce_fusion = f32[8,224]{1,0:T(8,128)S(1)} fusion(bf16[8,224,2048]{2,1,0:T(8,128)(2,1)} %get-tuple-element.15), kind=kLoop, calls=%fused_computation.1 | loop fusion | flops 11008256 | bytes 7347200 | tf_op jit(solution)/shard_map/reduce_sum | solution.py:619
  155.2 0.1 rsqrt.13
  155.3 0.1 dynamic-slice.1
  155.4 0.0 copy-start.3
  155.4 10.2 %bitcast_convert_fusion = f32[1792,2048]{1,0:T(8,128)} fusion(bf16[8,224,2048]{2,1,0:T(8,128)(2,1)} %get-tuple-element.15), kind=kLoop, calls=%fused_computation.49 | loop fusion | flops 3670016 | bytes 22020096 | tf_op jit(solution)/shard_map/convert_element_type | solution.py:618
  165.5 0.0 copy-done.3
  165.6 2.0 fusion.30
  167.5 3.3 %fusion.9.shared = f32[224,2048]{1,0:T(8,128)S(1)} fusion(bf16[256,2048]{1,0:T(8,128)(2,1)} %bitcast.47, bf16[2048,256]{1,0:T(8,128)(2,1)} %bitcast.49, f32[224,256]{1,0:T(8,128)S(1)} %fusion.30, f32[1792,2048]{1,0:T(8,128)} %bitcast_convert_fusion, s32[]{:T(128)S(6)} %select_n.12, f32[224]{0:T(256)S(1)} %dynamic-slice.1), kind=kOutput, calls=%fused_computation.18 | convolution fusion | flops 471023616 | bytes 5997444 | tf_op jit(solution)/shard_map/dot_general | solution.py:631
  170.8 4.3 %multiply_convert_fusion = bf16[8,224,2048]{2,1,0:T(8,128)(2,1)S(1)} fusion(f32[8,224]{1,0:T(8,128)S(1)} %add_rsqrt_fusion, bf16[8,224,2048]{2,1,0:T(8,128)(2,1)} %get-tuple-element.15), kind=kLoop, calls=%fused_computation | loop fusion | flops 11010048 | bytes 14687232 | tf_op jit(solution)/shard_map/convert_element_type | solution.py:619
  175.2 0.0 copy-start
  175.2 5.5 %fusion.14 = f32[1792,256]{0,1:T(8,128)} fusion(bf16[1792,2048]{1,0:T(8,128)(2,1)S(1)} %bitcast.41, bf16[2,2048,256]{2,1,0:T(8,128)(2,1)} %get-tuple-element.37), kind=kOutput, calls=%fused_computation.23 | convolution fusion | flops 1879048192 | bytes 10223616 | tf_op jit(solution)/shard_map/dot_general | solution.py:625
  180.7 0.0 copy-done
  180.7 0.8 dynamic-slice_bitcast_fusion
  181.6 0.1 reshape.76
  181.7 0.0 copy-start.1
  181.7 0.0 copy-start.8
  181.7 6.4 %fusion.2 = bf16[1792,256]{0,1:T(8,128)(2,1)S(1)} fusion(bf16[1792,2048]{1,0:T(8,128)(2,1)} %bitcast.42, f32[1792,256]{0,1:T(8,128)} %fusion.14, bf16[2,2048,256]{2,1,0:T(8,128)(2,1)} %get-tuple-element.38, f32[1792]{0:T(1024)S(1)} %get-tuple-element.23), kind=kOutput, calls=%fused_computation.9 | convolution fusion | flops 1882259456 | bytes 11148288 | tf_op jit(solution)/shard_map/dot_general | solution.py:625
  188.2 0.0 copy-done.1
  188.2 0.1 copy-done.8
  188.3 0.0 copy-start.7
  188.3 2.3 fusion.11
  190.7 0.0 copy-done.7
  190.7 0.0 copy-start.6
  190.7 2.4 fusion.3
  193.1 0.0 copy-done.6
  193.1 4.3 %convolution_convert_fusion = bf16[1792,2048]{1,0:T(8,128)(2,1)S(1)} fusion(bf16[512,2048]{1,0:T(8,128)(2,1)S(1)} %bitcast.51, bf16[1792,256]{0,1:T(8,128)(2,1)S(1)} %fusion.3, bf16[1792,256]{0,1:T(8,128)(2,1)S(1)} %fusion.2), kind=kOutput, calls=%fused_computation.2 | convolution fusion | flops 3765436416 | bytes 11272192 | tf_op jit(solution)/shard_map/dot_general | solution.py:630
  197.3 70.5 %shard_map.154 = bf16[224,1024]{1,0:T(8,128)(2,1)S(1)} custom-call(bf16[8,224,2048]{2,1,0:T(8,128)(2,1)S(1)} %bitcast.40, f32[224,2048]{1,0:T(8,128)S(1)} %fusion.9.shared), custom_call_target="tpu_custom_call" | custom-call | flops 200000000 | bytes 20000000 | tf_op jit(solution)/shard_map/pallas_call | solution.py:560
  267.9 0.8 copy.30
  268.7 1.3 copy.31
  270.0 1.3 copy.32
  271.3 0.0 copy-start.5
  271.3 1.3 copy.33
  272.6 0.0 copy-start.4
  272.6 1.0 copy.34
  273.6 0.0 copy-done.5
  273.6 1.0 copy.35
  274.6 0.0 copy-done.4
  274.6 1.0 copy.36
  (4 shorter events, 0.1 us)
Async XLA Ops:
  0.6 6.7 %copy-start.14 = (f32[256]{0:T(256)S(1)}, f32[256]{0:T(256)}, u32[]{:S(2)}) copy-start(f32[256]{0:T(256)} %param.13) | copy-start | bytes 3076
  0.6 6.7 %copy-start.11 = (f32[256,256]{1,0:T(8,128)S(1)}, f32[256,256]{1,0:T(8,128)}, u32[]{:S(2)}) copy-start(f32[256,256]{1,0:T(8,128)} %param.17) | copy-start | bytes 786436
  0.7 6.7 %copy-start.10 = (f32[256,256]{1,0:T(8,128)S(1)}, f32[256,256]{1,0:T(8,128)}, u32[]{:S(2)}) copy-start(f32[256,256]{1,0:T(8,128)} %param.18) | copy-start | bytes 786436
  0.7 7.5 %copy-start.2 = (f32[16,64,1024]{2,1,0:T(8,128)S(1)}, f32[16,64,1024]{2,1,0:T(8,128)}, u32[]{:S(2)}) copy-start(f32[16,64,1024]{2,1,0:T(8,128)} %param.16) | copy-start | bytes 12582916
  8.2 1.7 copy-start.9
  8.2 2.3 copy-start.12
  8.2 2.3 copy-start.13
  155.4 10.2 %copy-start.3 = (bf16[1,2048,256]{2,1,0:T(8,128)(2,1)S(1)}, bf16[1,2048,256]{2,1,0:T(8,128)(2,1)}, u32[]{:S(2)}) copy-start(bf16[1,2048,256]{2,1,0:T(8,128)(2,1)} %get-tuple-element.20) | copy-start | bytes 3145732
  175.2 5.5 %copy-start = (bf16[8,224,2048]{2,1,0:T(8,128)(2,1)}, bf16[8,224,2048]{2,1,0:T(8,128)(2,1)S(1)}, u32[]{:S(2)}) copy-start(bf16[8,224,2048]{2,1,0:T(8,128)(2,1)S(1)} %multiply_convert_fusion) | copy-start | bytes 22020100
  181.7 6.5 %copy-start.1 = (bf16[8,224,2048]{2,1,0:T(8,128)(2,1)S(1)}, bf16[8,224,2048]{2,1,0:T(8,128)(2,1)}, u32[]{:S(2)}) copy-start(bf16[8,224,2048]{2,1,0:T(8,128)(2,1)} %copy-done) | copy-start | bytes 22020100
  181.7 6.6 %copy-start.8 = (bf16[2,2048,256]{2,1,0:T(8,128)(2,1)S(1)}, bf16[2,2048,256]{2,1,0:T(8,128)(2,1)}, u32[]{:S(2)}) copy-start(bf16[2,2048,256]{2,1,0:T(8,128)(2,1)} %get-tuple-element.37) | copy-start | bytes 6291460
  188.3 2.4 copy-start.7
  190.7 2.4 copy-start.6
  271.3 2.3 copy-start.5
  272.6 1.9 copy-start.4

commit v2 on v1

--- a/solution.py
+++ b/solution.py
@@ -1,4 +1,6 @@
 import functools
+import math
+from types import SimpleNamespace
 
 import jax
 import jax.numpy as jnp
@@ -10,18 +12,14 @@
 MESH = pl.DeviceIdType.MESH
 
 
-def move_kernel(sizes, *refs):
+def plan(sizes, tok_in, sc_in, srcs, tok, sc, outs, sems):
     groups, n, tps = sizes
     chips, band = n // 2, n // tps
     half = band // 2
-    tok_in, sc_in = refs[:2]
-    srcs = refs[2:8]
-    tok, sc = refs[8:10]
-    outs = refs[10:16]
     (
         own_s, lz_s, lz_r, ls_s, ls_r, lx_s, lx_r, ly_s, ly_r,
         e_s, e_r, p_s, p_r, d_s, d_r, dy_s, dy_r, ds_s, ds_r,
-    ) = refs[16:]
+    ) = sems
     grp, fs, tp = lax.axis_index("grp"), lax.axis_index("fs"), lax.axis_index("tp")
     z, c = fs // 2, lax.rem(fs, 2)
     home = fs // band
@@ -230,40 +228,16 @@
             block if source is None else source, block, ds_s.at[q, x, v], ds_r.at[q, x, v], at(grp, both, tp)
         )
 
-    for copy in own:
-        copy.wait()
-    for i in (0, 1, 2, 3):
-        line_own(i)
-    for s in range(chips - 1):
-        for k in (0, 1):
-            for dc in (0, 1):
-                e_send(k, far(s) * 2 + dc, grp).start()
-    for k in (0, 1):
-        e_send(k, both, None).start()
-    for x in range(1, tps):
-        x_send(z, x).start()
-    for i in (0, 1, 2, 3):
-        for v in range(ways(i)):
-            if i or not v:
-                sib_send(i, z, v, own_share(i, v)).start()
-
-    @pl.when(home == tp)
-    def _():
-        e_send(2, both, None).start()
-        sd_sib(lax.rem(z, half), tp, 0, True, srcs[5].at[:, :, :]).start()
-
-    @pl.when(home != tp)
-    def _():
-        for dc in (0, 1):
-            e_send(2, z * 2 + dc, None).start()
-        sd_send(z, None).start()
-
-    for i in (0, 1, 2, 3):
-        line_arrivals(i, 1)
-    for s in range(chips - 1):
-        for dc in (0, 1):
-            e_send(2, far(s) * 2 + dc, grp).start()
-        sd_send(far(s), grp).start()
+
+    def sd_sources():
+        for q in range(half):
+            for x in range(tps):
+                yield q, x, tp * half + q
+
+    def downs(k):
+        for q, x, zs in sd_sources():
+            for dc in (0, 1) if k == 2 else (c,):
+                yield q, x, zs == z, zs * 2 + dc
 
     def keep(k, x):
         rows, wide = srcs[k].shape[1:]
@@ -274,182 +248,542 @@
             else:
                 outs[k][j, span(fs, rows), :] = srcs[k][first + j]
 
-    for k in (0, 1, 3, 4):
-        keep(k, tp)
-
-    @pl.when(home == tp)
-    def _():
-        keep(2, tp)
-        keep(5, tp)
-
-    for k in (0, 1):
+    def keep_all():
+        for k in (0, 1, 3, 4):
+            keep(k, tp)
+
+        @pl.when(home == tp)
+        def _():
+            keep(2, tp)
+            keep(5, tp)
+
+    def near_sends(lines):
+        for k in (0, 1):
+            e_send(k, both, None).start()
+        for x in range(1, tps):
+            x_send(z, x).start()
+        for i in lines:
+            for v in range(ways(i)):
+                if i or not v:
+                    sib_send(i, z, v, own_share(i, v)).start()
+
+    def near_downs():
+        @pl.when(home == tp)
+        def _():
+            e_send(2, both, None).start()
+            sd_sib(lax.rem(z, half), tp, 0, True, srcs[5].at[:, :, :]).start()
+
+        @pl.when(home != tp)
+        def _():
+            for dc in (0, 1):
+                e_send(2, z * 2 + dc, None).start()
+            sd_send(z, None).start()
+
+    def rows_out(s):
+        for k in (0, 1):
+            for dc in (0, 1):
+                e_send(k, far(s) * 2 + dc, grp).start()
+
+    def rows_in(s):
+        for dc in (0, 1):
+            for k in (0, 1):
+                e_arrive(k, far(s) * 2 + dc, tp, False)
+
+    def downs_out():
         for s in range(chips - 1):
             for dc in (0, 1):
-                e_arrive(k, far(s) * 2 + dc, tp, False)
-    for d in range(2, chips):
-        for i in (0, 1, 2, 3):
-            line_arrivals(i, d)
-
-    def sd_sources():
-        for q in range(half):
-            for x in range(tps):
-                yield q, x, tp * half + q
-
-    def downs(k):
-        for q, x, zs in sd_sources():
-            near = zs == z
-            cores = (0, 1) if k == 2 else (0,)
-            for dc in cores:
-                f = zs * 2 + (dc if k == 2 else c)
-                yield q, x, near, f
-
-    for q, x, near, f in downs(2):
-        @pl.when(jnp.logical_not(near))
-        def _():
-            e_arrive(2, f, x, False)
-
-        @pl.when(jnp.logical_and(near, jnp.logical_or(f != fs, tp != x)))
-        def _():
-            e_arrive(2, f, x, True)
-
-    for q, x, near, f in downs(5):
-        @pl.when(jnp.logical_not(near))
-        def _():
-            arrived(down_block(5, f, x, grp), d_r.at[q, x])
-            sd_sib(q, x, 0, False).start()
-            for y in range(1, groups):
-                sd_pass(q, x, y).start()
-
-        @pl.when(jnp.logical_and(near, tp != x))
-        def _():
-            arrived(down_block(5, f, x, None), d_r.at[q, x])
-            sd_sib(q, x, 0, True).start()
-
-    for zs in range(chips):
+                e_send(2, far(s) * 2 + dc, grp).start()
+
+    def sds_out():
+        for s in range(chips - 1):
+            sd_send(far(s), grp).start()
+
+    def downs_in(want):
+        for q, x, near, f in downs(2):
+            if q * tps + x not in want:
+                continue
+
+            @pl.when(jnp.logical_not(near))
+            def _():
+                e_arrive(2, f, x, False)
+
+            @pl.when(jnp.logical_and(near, jnp.logical_or(f != fs, tp != x)))
+            def _():
+                e_arrive(2, f, x, True)
+
+    def sds_in():
+        for q, x, near, f in downs(5):
+            @pl.when(jnp.logical_not(near))
+            def _():
+                arrived(down_block(5, f, x, grp), d_r.at[q, x])
+                sd_sib(q, x, 0, False).start()
+                for y in range(1, groups):
+                    sd_pass(q, x, y).start()
+
+            @pl.when(jnp.logical_and(near, tp != x))
+            def _():
+                arrived(down_block(5, f, x, None), d_r.at[q, x])
+                sd_sib(q, x, 0, True).start()
+
+    def x_in(zs):
         for x in range(1, tps):
             arrived(x_block(zs * 2 + c, x), lx_r.at[x - 1, zs])
             sib_send(0, zs, x).start()
-    for dz in range(1, chips):
-        zs = turn(z, dz, chips)
-        for i in (2, 3):
-            for y in range(1, groups):
-                arrived(sib_block(i, zs * 2 + c, y), ly_r.at[i - 2, y - 1, zs])
-                sib_send(i, zs, y).start()
-    for q, x, near, f in downs(5):
-        @pl.when(jnp.logical_not(near))
-        def _():
-            for y in range(1, groups):
-                arrived(down_block(5, f, x, turn(grp, -y, groups)), dy_r.at[q, x, y - 1])
-                sd_sib(q, x, y, False).start()
-
-    for k in (0, 1):
-        arrived(e_dst(k, both, tp, None), e_r.at[k, e_slot(k, both, tp)])
-        for s in range(chips - 1):
-            for dc in (0, 1):
-                e_settle(k, far(s) * 2 + dc, tp)
-    for q, x, near, f in downs(2):
-        @pl.when(jnp.logical_not(near))
-        def _():
-            e_settle(2, f, x)
-    for zs in range(chips):
-        for i in (0, 1, 2, 3):
+
+    def x_arrivals(d):
+        if not d:
+            x_in(z)
+            return
+        for up in (1, 0):
+            @pl.when(z >= d if up else z + d < chips)
+            def _():
+                x_in(turn(z, -d if up else d, chips))
+
+    def shared_y():
+        for dz in range(1, chips):
+            zs = turn(z, dz, chips)
+            for i in (2, 3):
+                for y in range(1, groups):
+                    arrived(sib_block(i, zs * 2 + c, y), ly_r.at[i - 2, y - 1, zs])
+                    sib_send(i, zs, y).start()
+        for q, x, near, f in downs(5):
+            @pl.when(jnp.logical_not(near))
+            def _():
+                for y in range(1, groups):
+                    arrived(down_block(5, f, x, turn(grp, -y, groups)), dy_r.at[q, x, y - 1])
+                    sd_sib(q, x, y, False).start()
+
+    def rows_settled():
+        for k in (0, 1):
+            arrived(e_dst(k, both, tp, None), e_r.at[k, e_slot(k, both, tp)])
+            for s in range(chips - 1):
+                for dc in (0, 1):
+                    e_settle(k, far(s) * 2 + dc, tp)
+
+    def downs_settled():
+        for q, x, near, f in downs(2):
+            @pl.when(jnp.logical_not(near))
+            def _():
+                e_settle(2, f, x)
+
+    def line_settled(i):
+        for zs in range(chips):
             for v in range(ways(i)):
                 arrived(sib_block(i, zs * 2 + 1 - c, v), ls_r.at[i, v, zs])
-    for q, x, near, f in downs(5):
-        other = f + 1 - 2 * c
-        @pl.when(near)
+
+    def sds_settled():
+        for q, x, near, f in downs(5):
+            other = f + 1 - 2 * c
+
+            @pl.when(near)
+            def _():
+                arrived(down_block(5, other, x, None), ds_r.at[q, x, 0])
+
+            @pl.when(jnp.logical_not(near))
+            def _():
+                for v in range(groups):
+                    arrived(down_block(5, other, x, turn(grp, -v, groups)), ds_r.at[q, x, v])
+
+    def sent():
+        for zs in range(chips):
+            for i in (0, 1, 2, 3):
+                for v in range(ways(i)):
+                    sib_send(i, zs, v).wait_send()
+            for x in range(1, tps):
+                x_send(zs, x).wait_send()
+        for dz in range(1, chips):
+            for i in (2, 3):
+                for y in range(1, groups):
+                    y_send(i, turn(z, dz, chips), y).wait_send()
+        for d in range(chips):
+            for up in (0, 1):
+                @pl.when(jnp.logical_and(ends(up), z >= d if up else z + d < chips))
+                def _():
+                    for i in (0, 1, 2, 3):
+                        line_send(i, turn(z, -d if up else d, chips), up).wait_send()
+        for k in (0, 1):
+            e_send(k, both, None).wait_send()
+        for s in range(chips - 1):
+            for k in (0, 1, 2):
+                for dc in (0, 1):
+                    e_send(k, far(s) * 2 + dc, grp).wait_send()
+            sd_send(far(s), grp).wait_send()
+
+        @pl.when(home == tp)
         def _():
-            arrived(down_block(5, other, x, None), ds_r.at[q, x, 0])
-
-        @pl.when(jnp.logical_not(near))
+            e_send(2, both, None).wait_send()
+
+        @pl.when(home != tp)
         def _():
-            for v in range(groups):
-                arrived(down_block(5, other, x, turn(grp, -v, groups)), ds_r.at[q, x, v])
-
-    for zs in range(chips):
-        for i in (0, 1, 2, 3):
-            for v in range(ways(i)):
-                sib_send(i, zs, v).wait_send()
-        for x in range(1, tps):
-            x_send(zs, x).wait_send()
-    for dz in range(1, chips):
+            for dc in (0, 1):
+                e_send(2, z * 2 + dc, None).wait_send()
+            sd_send(z, None).wait_send()
+
+        for q, x, near, f in downs(5):
+            @pl.when(near)
+            def _():
+                sd_sib(q, x, 0, True).wait_send()
+
+            @pl.when(jnp.logical_not(near))
+            def _():
+                for v in range(groups):
+                    sd_sib(q, x, v, False).wait_send()
+                for y in range(1, groups):
+                    sd_pass(q, x, y).wait_send()
+
+    for copy in own:
+        copy.wait()
+    return SimpleNamespace(**locals())
+
+
+def move_kernel(sizes, *refs):
+    chips = sizes[1] // 2
+    m = plan(sizes, refs[0], refs[1], refs[2:8], refs[8], refs[9], refs[10:16], refs[16:])
+    for i in (0, 1):
+        m.line_own(i)
+    m.rows_out(0)
+    m.near_sends((0, 1, 2, 3))
+    m.near_downs()
+    for d in range(1, chips):
+        m.line_arrivals(0, d)
+        m.line_arrivals(1, d)
+        m.rows_out(d) if d < chips - 1 else None
+    m.downs_out()
+    for i in (2, 3):
+        m.line_own(i)
+    m.sds_out()
+    m.keep_all()
+    for s in range(chips - 1):
+        m.rows_in(s)
+    for d in range(chips):
+        m.x_arrivals(d)
+    for d in range(1, chips):
         for i in (2, 3):
-            for y in range(1, groups):
-                y_send(i, turn(z, dz, chips), y).wait_send()
-    for d in range(chips):
-        for up in (0, 1):
-            @pl.when(jnp.logical_and(ends(up), z >= d if up else z + d < chips))
-            def _():
-                for i in (0, 1, 2, 3):
-                    line_send(i, turn(z, -d if up else d, chips), up).wait_send()
-    for k in (0, 1):
-        e_send(k, both, None).wait_send()
-    for s in range(chips - 1):
-        for k in (0, 1, 2):
-            for dc in (0, 1):
-                e_send(k, far(s) * 2 + dc, grp).wait_send()
-        sd_send(far(s), grp).wait_send()
-
-    @pl.when(home == tp)
-    def _():
-        e_send(2, both, None).wait_send()
-
-    @pl.when(home != tp)
-    def _():
-        for dc in (0, 1):
-            e_send(2, z * 2 + dc, None).wait_send()
-        sd_send(z, None).wait_send()
-
-    for q, x, near, f in downs(5):
-        @pl.when(near)
-        def _():
-            sd_sib(q, x, 0, True).wait_send()
-
-        @pl.when(jnp.logical_not(near))
-        def _():
-            for v in range(groups):
-                sd_sib(q, x, v, False).wait_send()
-            for y in range(1, groups):
-                sd_pass(q, x, y).wait_send()
-
-
-def move(sizes, tokens, scales, gate, up, down, shared_gate, shared_up, shared_down):
+            m.line_arrivals(i, d)
+    m.downs_in(range(sizes[1]))
+    m.sds_in()
+    m.shared_y()
+    m.rows_settled()
+    m.downs_settled()
+    for i in (0, 1, 2, 3):
+        m.line_settled(i)
+    m.sds_settled()
+    m.sent()
+
+
+def fused_kernel(sizes, *refs):
     groups, n, tps = sizes
     chips = n // 2
-    half = n // tps // 2
+    bf16, f32 = jnp.bfloat16, jnp.float32
+    out, outs = refs[8], refs[9:15]
+    tok, sc, nb, act, mine, theirs, near, across, summed, zr, extra, hs = refs[15:27]
+    near_s, near_r, x_s, x_r, z_s, z_r = refs[27:33]
+    m = plan(sizes, refs[0], refs[1], refs[2:8], tok, sc, outs, refs[33:])
+    z, c, tp, fs, grp = m.z, m.c, m.tp, m.fs, m.grp
+    gate, up, down, sg, su, sd = outs
+    held, _, hid = gate.shape
+    count, cols = out.shape
+    width = cols * tps
+
+    for i in (0, 1):
+        m.line_own(i)
+    m.rows_out(0)
+    m.near_sends((0, 1))
+    m.near_downs()
+    for d in range(1, chips):
+        m.line_arrivals(0, d)
+        m.line_arrivals(1, d)
+        if d < chips - 1:
+            m.rows_out(d)
+        m.x_arrivals(d - 1)
+    m.downs_out()
+    for i in (2, 3):
+        m.line_own(i)
+        for v in range(groups):
+            m.sib_send(i, z, v, m.own_share(i, v)).start()
+    m.sds_out()
+    m.keep_all()
+    for s in range(chips - 1):
+        m.rows_in(s)
+    m.x_arrivals(chips - 1)
+    m.rows_settled()
+    m.line_settled(0)
+    m.line_settled(1)
+
+    step = 32
+
+    def norm(f):
+        @pl.loop(0, count // step)
+        def _(i):
+            r = pl.ds(pl.multiple_of(i * step, step), step)
+            wide = tok[f, r, :].astype(f32)
+            mean = jnp.mean(wide * wide, axis=1, keepdims=True)
+            nb[r, :] = (wide * lax.rsqrt(mean + 1e-06)).astype(bf16)
+
+    def hidden(g, u):
+        gated = jnp.dot(nb[...], g, preferred_element_type=f32)
+        return jax.nn.silu(gated) * jnp.dot(nb[...], u, preferred_element_type=f32)
+
+    def active(f):
+        norm(f)
+        columns = sc[f].T[:count]
+        lane = lax.broadcasted_iota(jnp.int32, columns.shape, 1)
+        for j in range(held):
+            scale = jnp.sum(jnp.where(lane == fs * held + j, columns, 0.0), axis=1, keepdims=True)
+            act[f, :, j * hid:(j + 1) * hid] = (hidden(gate[j], up[j]) * scale).astype(bf16)
+
+    parts = m.half * tps
+    for p in range(parts):
+        lo, hi = n * p // parts, n * (p + 1) // parts
+
+        @pl.loop(lo, hi)
+        def _(f):
+            active(f)
+
+        m.downs_in((p,))
+    m.downs_settled()
+
+    def goal(s):
+        return m.far(s) if s < chips - 1 else z
+
+    chunk = min(512, width)
+
+    def product(f, to, s):
+        @pl.loop(0, width // chunk)
+        def _(j):
+            at_j = m.span(j, chunk)
+            total = jnp.dot(act[f, :, :hid], down[0, :, at_j], preferred_element_type=f32)
+            for e in range(1, held):
+                total = total + jnp.dot(act[f, :, e * hid:(e + 1) * hid], down[e, :, at_j], preferred_element_type=f32)
+            to[s, :, at_j] = total.astype(bf16)
+
+    def near_copy(s):
+        return m.remote(theirs.at[s], near.at[s], near_s.at[s], near_r.at[s], m.at(grp, m.both, tp))
+
+    def x_copy(s, x):
+        there = m.turn(tp, x, tps)
+        return m.remote(
+            mine.at[s, :, m.span(there, cols)], across.at[x - 1, s], x_s.at[x - 1, s], x_r.at[x - 1, s], m.at(grp, fs, there)
+        )
+
+    def z_copy(s, zd, rising):
+        there = m.turn(z, 1 if rising else -1, chips) * 2 + c
+        return m.remote(
+            summed.at[s], zr.at[rising, zd], z_s.at[s], z_r.at[rising, zd], m.at(grp, there, tp)
+        )
+
+    def produce(s):
+        product(goal(s) * 2 + 1 - c, theirs, s)
+        near_copy(s).start()
+        product(goal(s) * 2 + c, mine, s)
+
+    def meet(s, extra=None):
+        near_copy(s).wait_recv()
+
+        @pl.loop(0, count // step)
+        def _(i):
+            r = pl.ds(pl.multiple_of(i * step, step), step)
+            total = mine[s, r, :].astype(f32) + near[s, r, :].astype(f32)
+            if extra is not None:
+                total = total + extra[r, :]
+            mine[s, r, :] = total.astype(bf16)
+
+        for x in range(1, tps):
+            x_copy(s, x).start()
+
+    here = m.span(tp, cols)
+
+    def total_of(s, r):
+        total = mine[s, r, here].astype(f32)
+        for x in range(1, tps):
+            total = total + across[x - 1, s, r, :].astype(f32)
+        return total
+
+    def x_met(s):
+        for x in range(1, tps):
+            x_copy(s, x).wait_recv()
+
+    def onward(s):
+        zd = goal(s)
+        x_met(s)
+        for rising in (1, 0):
+            @pl.when(zd > z if rising else zd < z)
+            def _():
+                behind = z > 0 if rising else z < chips - 1
+
+                @pl.when(behind)
+                def _():
+                    m.arrived(zr.at[rising, zd], z_r.at[rising, zd])
+
+                    @pl.loop(0, count // step)
+                    def _(i):
+                        r = pl.ds(pl.multiple_of(i * step, step), step)
+                        summed[s, r, :] = (total_of(s, r) + zr[rising, zd, r, :].astype(f32)).astype(bf16)
+
+                @pl.when(jnp.logical_not(behind))
+                def _():
+                    @pl.loop(0, count // step)
+                    def _(i):
+                        r = pl.ds(pl.multiple_of(i * step, step), step)
+                        summed[s, r, :] = total_of(s, r).astype(bf16)
+
+                z_copy(s, zd, rising).start()
+
+    produce(0)
+    for s in range(1, chips):
+        produce(s)
+        meet(s - 1)
+
+    for d in range(1, chips):
+        for i in (2, 3):
+            m.line_arrivals(i, d)
+    m.sds_in()
+    m.shared_y()
+    for i in (2, 3):
+        m.line_settled(i)
+    m.sds_settled()
+    norm(fs)
+    hs[...] = hidden(sg[0], su[0]).astype(bf16)
+
+    @pl.loop(0, width // chunk)
+    def _(j):
+        at_j = m.span(j, chunk)
+        extra[:, at_j] = jnp.dot(hs[...], sd[0, :, at_j], preferred_element_type=f32)
+
+    meet(chips - 1, extra)
+    for s in range(chips - 1):
+        onward(s)
+    last = chips - 1
+    x_met(last)
+    for rising in (1, 0):
+        @pl.when(z > 0 if rising else z < chips - 1)
+        def _():
+            m.arrived(zr.at[rising, z], z_r.at[rising, z])
+
+    @pl.loop(0, count // step)
+    def _(i):
+        r = pl.ds(pl.multiple_of(i * step, step), step)
+        extra[r, :cols] = total_of(last, r)
+
+    for rising in (1, 0):
+        @pl.when(z > 0 if rising else z < chips - 1)
+        def _():
+            @pl.loop(0, count // step)
+            def _(i):
+                r = pl.ds(pl.multiple_of(i * step, step), step)
+                extra[r, :cols] = extra[r, :cols] + zr[rising, z, r, :].astype(f32)
+
+    @pl.loop(0, count // step)
+    def _(i):
+        r = pl.ds(pl.multiple_of(i * step, step), step)
+        out[r, :] = extra[r, :cols].astype(bf16)
+
+    for s in range(chips):
+        near_copy(s).wait_send()
+        for x in range(1, tps):
+            x_copy(s, x).wait_send()
+        if s < chips - 1:
+            zd = goal(s)
+            for rising in (1, 0):
+                @pl.when(zd > z if rising else zd < z)
+                def _():
+                    z_copy(s, zd, rising).wait_send()
+    m.sent()
+
+
+def moved_shapes(sizes, gate, up, down, shared_gate, shared_up, shared_down):
+    _, n, tps = sizes
     held = gate.shape[0] // n
-    bf16 = jnp.bfloat16
-    ways = max(groups, tps)
 
     def rows(a, lead):
-        return jax.ShapeDtypeStruct((lead, n * a.shape[1], a.shape[2]), bf16)
+        return jax.ShapeDtypeStruct((lead, n * a.shape[1], a.shape[2]), jnp.bfloat16)
 
     def downs(a, lead):
-        return jax.ShapeDtypeStruct((lead, n // tps * a.shape[1], tps * a.shape[2]), bf16)
-
+        return jax.ShapeDtypeStruct((lead, n // tps * a.shape[1], tps * a.shape[2]), jnp.bfloat16)
+
+    return [
+        rows(gate, held), rows(up, held), downs(down, held),
+        rows(shared_gate, 1), rows(shared_up, 1), downs(shared_down, 1),
+    ]
+
+
+def plan_sems(sizes):
+    groups, n, tps = sizes
+    chips, half, ways = n // 2, n // tps // 2, max(groups, tps)
     dma = pltpu.SemaphoreType.DMA
+    return [
+        dma((2,)), dma((4, 2, chips)), dma((4, chips)), dma((4, ways, chips)), dma((4, ways, chips)),
+        dma((tps - 1, chips)), dma((tps - 1, chips)), dma((2, groups - 1, chips)), dma((2, groups - 1, chips)),
+        dma((3, n)), dma((3, n)), dma((3, n, groups - 1)), dma((3, n, groups - 1)),
+        dma((chips,)), dma((half, tps)), dma((half, tps, groups - 1)), dma((half, tps, groups - 1)),
+        dma((half, tps, groups)), dma((half, tps, groups)),
+    ]
+
+
+def token_shapes(sizes, tokens, scales):
+    n, tps = sizes[1:]
+    return (n, tokens.shape[0], tps * tokens.shape[1]), (n,) + scales.shape
+
+
+def move(sizes, tokens, scales, *weights):
+    tok, sc = token_shapes(sizes, tokens, scales)
     return pl.pallas_call(
         functools.partial(move_kernel, sizes),
-        out_shape=(
-            jax.ShapeDtypeStruct((n, tokens.shape[0], tps * tokens.shape[1]), bf16),
-            jax.ShapeDtypeStruct((n,) + scales.shape, jnp.float32),
-            rows(gate, held), rows(up, held), downs(down, held),
-            rows(shared_gate, 1), rows(shared_up, 1), downs(shared_down, 1),
-        ),
+        out_shape=[jax.ShapeDtypeStruct(tok, jnp.bfloat16), jax.ShapeDtypeStruct(sc, jnp.float32)]
+        + moved_shapes(sizes, *weights),
         in_specs=[pl.BlockSpec(memory_space=pl.ANY)] * 2 + [pl.BlockSpec(memory_space=pltpu.VMEM)] * 6,
         out_specs=[pl.BlockSpec(memory_space=pltpu.VMEM)] * 8,
-        scratch_shapes=[
-            dma((2,)), dma((4, 2, chips)), dma((4, chips)), dma((4, ways, chips)), dma((4, ways, chips)),
-            dma((tps - 1, chips)), dma((tps - 1, chips)), dma((2, groups - 1, chips)), dma((2, groups - 1, chips)),
-            dma((3, n)), dma((3, n)), dma((3, n, groups - 1)), dma((3, n, groups - 1)),
-            dma((chips,)), dma((half, tps)), dma((half, tps, groups - 1)), dma((half, tps, groups - 1)),
-            dma((half, tps, groups)), dma((half, tps, groups)),
-        ],
+        scratch_shapes=plan_sems(sizes),
         compiler_params=pltpu.CompilerParams(
             collective_id=0, has_side_effects=True, vmem_limit_bytes=60 * 1024 * 1024
         ),
         cost_estimate=pl.CostEstimate(flops=400_000_000, bytes_accessed=20_000_000, transcendentals=0),
-    )(tokens, scales, gate, up, down, shared_gate, shared_up, shared_down)
+    )(tokens, scales, *weights)
+
+
+def fused_scratch(sizes, tokens, scales, gate, shared_gate):
+    _, n, tps = sizes
+    chips = n // 2
+    count, cols = tokens.shape
+    width = cols * tps
+    tok, sc = token_shapes(sizes, tokens, scales)
+    held, hid = gate.shape[0] // n, gate.shape[2]
+    bf16, f32 = jnp.bfloat16, jnp.float32
+    return [
+        (tok, bf16), (sc, f32), ((count, width), bf16), ((n, count, held * hid), bf16),
+        ((chips, count, width), bf16), ((chips, count, width), bf16), ((chips, count, width), bf16),
+        ((tps - 1, chips, count, cols), bf16), ((chips, count, cols), bf16), ((2, chips, count, cols), bf16),
+        ((count, width), f32), ((count, shared_gate.shape[2]), bf16),
+    ]
+
+
+def size_of(shape, dtype):
+    return math.prod(shape) * jnp.dtype(dtype).itemsize
+
+
+def fused_fits(sizes, tokens, scales, *weights):
+    total = sum(size_of(*s) for s in fused_scratch(sizes, tokens, scales, weights[0], weights[3]))
+    total += sum(size_of(s.shape, s.dtype) for s in moved_shapes(sizes, *weights)) + sum(size_of(w.shape, w.dtype) for w in weights)
+    return total + 2 * size_of(tokens.shape, tokens.dtype) < 54 * 2**20
+
+
+def fused(sizes, tokens, scales, *weights):
+    _, n, tps = sizes
+    chips = n // 2
+    dma = pltpu.SemaphoreType.DMA
+    return pl.pallas_call(
+        functools.partial(fused_kernel, sizes),
+        out_shape=[jax.ShapeDtypeStruct(tokens.shape, jnp.bfloat16)] + moved_shapes(sizes, *weights),
+        in_specs=[pl.BlockSpec(memory_space=pl.ANY)] * 2 + [pl.BlockSpec(memory_space=pltpu.VMEM)] * 6,
+        out_specs=[pl.BlockSpec(memory_space=pltpu.VMEM)] * 7,
+        scratch_shapes=[pltpu.VMEM(*s) for s in fused_scratch(sizes, tokens, scales, weights[0], weights[3])]
+        + [dma((chips,)), dma((chips,)), dma((tps - 1, chips)), dma((tps - 1, chips)), dma((chips,)), dma((2, chips))]
+        + plan_sems(sizes),
+        compiler_params=pltpu.CompilerParams(
+            collective_id=2, has_side_effects=True, vmem_limit_bytes=60 * 1024 * 1024
+        ),
+        cost_estimate=pl.CostEstimate(flops=12_000_000_000, bytes_accessed=20_000_000, transcendentals=0),
+    )(tokens, scales, *weights)
 
 
 def combine_kernel(sizes, part, shared, out, near, held, across, summed, far, local_sem, near_s, near_r, x_s, x_r, z_s, z_r):
@@ -601,10 +935,7 @@
     per_expert = jnp.sum(jnp.where(chosen, route_weights[:, :, None], 0.0), axis=1)
     count = tokens.shape[0]
     scales = jnp.pad(per_expert.T, ((0, 0), (0, -count % 128)))
-    moved = move(
-        sizes,
-        tokens,
-        scales,
+    weights = (
         (gate_experts * gain_rows).astype(bf16),
         (up_experts * gain_rows).astype(bf16),
         down_experts.astype(bf16),
@@ -612,6 +943,10 @@
         (shared_up[None] * gain_rows).astype(bf16),
         shared_down[None].astype(bf16),
     )
+    if fused_fits(sizes, tokens, scales, *weights):
+        mixed, gate_local, up_local, down_local, sg, su, sd = fused(sizes, tokens, scales, *weights)
+        return mixed, gate_local, up_local, down_local, sg[0], su[0], sd[0]
+    moved = move(sizes, tokens, scales, *weights)
     everyone, scales, gate_local, up_local, down_local, sg, su, sd = moved
     sg, su, sd = sg[0], su[0], sd[0]
     here = lax.axis_index("fs")

time: 276 us -> 237 us (0.86)
  matrix products: 26.2 us -> 0 us
  other arithmetic: 28.9 us -> 13.4 us
  local copies, waits for them, and re-layouts: 9.58 us -> 13.5 us
    dot_general x7 -> x0, matrix products: 26.2 us -> none  [the longest x3 9.82 us: hidden(): jnp.dot(x, g, preferred_element_type=f32)]
    convert_element_type x2 -> x0, other arithmetic: 14.5 us -> none  [the longest x1 10.2 us: per_device(): widened = everyone.reshape(n * count, width).astype(f32)]
    unnamed x37 -> x21, local copies, waits for them, and re-layouts: 7.83 us -> 12.9 us
    reduce_sum x1 -> x0, other arithmetic: 4.58 us -> none  [per_device(): jnp.mean(widened * widened, axis=1, keepdims=True) + 1e-06]
    pallas_call x2 -> x1, Pallas kernels: 210 us -> 209 us  [fused(): pl.pallas_call(functools.partial(fused_kernel, sizes), out_shape=[jax.Sha...]
where the time goes in v2:
time: 237 us
  Pallas kernels  209 us (88%)
  local copies, waits for them, and re-layouts  13.5 us (6%)
  other arithmetic  13.4 us (6%)
    pallas_call x1, Pallas kernels, fused(): pl.pallas_call(functools.partial(fused_kernel, sizes), out_shape=[jax.Sha...  209 us
    unnamed x21, local copies, waits for them, and re-layouts  12.9 us
    convert_element_type x1, other arithmetic, per_device(): (up_experts * gain_rows).astype(bf16)  5.23 us

profile of v2, /device:TPU:0, one launch (start us, length us, event | category | flops | bytes accessed | tf_op | source)
XLA Modules:
  0.0 236.7 jit_solution(8410624964096053300)
XLA Ops:
  0.6 0.7 select_reduce_fusion
  1.4 0.6 pad.4.refs_1_
  2.0 1.6 convert_bitcast_fusion.refs_7_
  3.6 1.8 fusion.1
  5.4 0.0 copy-start
  5.4 0.0 copy-start.6
  5.5 4.0 %convert_element_type.28.refs_4_ = bf16[16,64,1024]{2,1,0:T(8,128)(2,1)} convert(f32[16,64,1024]{2,1,0:T(8,128)} %param.16) | non-fusion elementwise | flops 1048576 | bytes 6291456 | tf_op jit(solution)/shard_map/convert_element_type | solution.py:941
  9.4 0.0 copy-done
  9.4 0.0 copy-done.6
  9.4 5.2 %multiply_convert_fusion = (bf16[16,256,256]{2,1,0:T(8,128)(2,1)}, bf16[16,256,256]{2,1,0:T(8,128)(2,1)}) fusion(f32[16,256,256]{2,1,0:T(8,128)S(1)} %copy-done, f32[256]{0:T(256)S(1)} %copy-done.6, f32[16,256,256]{2,1,0:T(8,128)} %param.14), kind=kLoop, calls=%fused_computation | loop fusion | flops 4194304 | bytes 12583936 | tf_op jit(solution)/shard_map/convert_element_type | solution.py:940
  14.7 209.2 %shard_map.153 = (bf16[224,1024]{1,0:T(8,128)(2,1)}, bf16[2,2048,256]{2,1,0:T(8,128)(2,1)}, bf16[2,2048,256]{2,1,0:T(8,128)(2,1)}, bf16[2,256,2048]{2,1,0:T(8,12...) custom-call(bf16[224,1024]{1,0:T(8,128)(2,1)} %refs_0_.1, ...), custom_call_target="tpu_custom_call" | custom-call | flops 12000000000 | bytes 20000000 | tf_op jit(solution)/shard_map/pallas_call | solution.py:774
  223.8 1.8 copy.26
  225.7 0.0 copy-start.2
  225.7 3.2 %copy.27 = bf16[2,2048,256]{2,1,0:T(8,128)(2,1)} copy(bf16[2,2048,256]{2,1,0:T(8,128)(2,1)} %get-tuple-element.33) | data formatting | bytes 4194304
  228.9 0.0 copy-done.2
  228.9 0.0 copy-start.1
  228.9 1.3 copy.28
  230.2 1.0 copy-done.1
  231.2 0.0 copy-start.5
  231.2 1.3 copy.29
  232.5 0.6 copy-done.5
  233.2 0.0 copy-start.4
  233.2 0.0 copy-start.3
  233.2 1.0 copy.30
  234.1 0.6 copy-done.4
  234.8 1.0 copy.31
  235.7 0.0 copy-done.3
  235.7 1.0 copy.32
Async XLA Ops:
  5.4 4.0 %copy-start = (f32[16,256,256]{2,1,0:T(8,128)S(1)}, f32[16,256,256]{2,1,0:T(8,128)}, u32[]{:S(2)}) copy-start(f32[16,256,256]{2,1,0:T(8,128)} %param.15) | copy-start | bytes 12582916
  5.4 4.0 %copy-start.6 = (f32[256]{0:T(256)S(1)}, f32[256]{0:T(256)}, u32[]{:S(2)}) copy-start(f32[256]{0:T(256)} %param.13) | copy-start | bytes 3076
  225.7 3.2 %copy-start.2 = (bf16[2,2048,256]{2,1,0:T(8,128)(2,1)S(1)}, bf16[2,2048,256]{2,1,0:T(8,128)(2,1)}, u32[]{:S(2)}) copy-start(bf16[2,2048,256]{2,1,0:T(8,128)(2,1)} %get-tuple-element.34) | copy-start | bytes 6291460
  228.9 2.3 copy-start.1
  231.2 2.0 copy-start.5
  233.2 1.6 copy-start.4
  233.2 2.6 %copy-start.3 = (bf16[1,256,2048]{2,1,0:T(8,128)(2,1)S(1)}, bf16[1,256,2048]{2,1,0:T(8,128)(2,1)}, u32[]{:S(2)}) copy-start(bf16[1,256,2048]{2,1,0:T(8,128)(2,1)} %get-tuple-element.20) | copy-start | bytes 3145732
